TPU v7x, 32 devices: a whole 2x2x4 slice. The times are simulated.
32 devices in a mesh: fs: 4 (over z), tp: 4 (over y, x), rep: 2 (over core).
Axes of the slice: x: 2, y: 2, z: 4, core: 2. Of those that a mesh axis runs over, the one named last changes fastest.
Arguments:
- gate_grads: float32 [2, 5632, 2048], P('rep', 'fs', 'tp'), may hold values from -16 to 16, as said below
- gate_velocity: float32 [5632, 2048], P(('fs', 'rep'), 'tp'), may hold values from -31 to 31, as said below
- gate_weight: float32 [5632, 2048], P(('fs', 'rep'), 'tp'), may hold values from -4 to 4
- up_grads: float32 [2, 5632, 2048], P('rep', 'fs', 'tp'), may hold values from -16 to 16, as said below
- up_velocity: float32 [5632, 2048], P(('fs', 'rep'), 'tp'), may hold values from -31 to 31, as said below
- up_weight: float32 [5632, 2048], P(('fs', 'rep'), 'tp'), may hold values from -4 to 4
- branch_grads: float32 [2, 2048, 1024], P('rep', 'fs', 'tp'), may hold values from -16 to 16, as said below
- branch_velocity: float32 [2048, 1024], P(('fs', 'rep'), 'tp'), may hold values from -31 to 31, as said below
- branch_weight: float32 [2048, 1024], P(('fs', 'rep'), 'tp'), may hold values from -4 to 4
Outputs:
- gate_momentum: float32 [5632, 2048], P(('fs', 'rep'), 'tp')
- gate_updated: float32 [5632, 2048], P(('fs', 'rep'), 'tp')
- up_momentum: float32 [5632, 2048], P(('fs', 'rep'), 'tp')
- up_updated: float32 [5632, 2048], P(('fs', 'rep'), 'tp')
- branch_momentum: float32 [2048, 1024], P(('fs', 'rep'), 'tp')
- branch_updated: float32 [2048, 1024], P(('fs', 'rep'), 'tp')
Inputs may be any that keep to these rules, and one draw needn't show every extreme that they name: `gate_grads`: entries vary in scale over rows and over columns. `up_grads`: entries vary in scale over rows and over columns. `branch_grads`: entries vary in scale over rows and over columns. `gate_velocity`: entries vary in scale over rows and over columns. `up_velocity`: entries vary in scale over rows and over columns. `branch_velocity`: entries vary in scale over rows and over columns.
All inputs are finite; a program needn't handle non-finite values.
Results may differ from a plain program's by a relative error of at most 0.039.
Values may be sent and summed in bfloat16 or wider, within the bound.
No kernel may reach another device: no remote copies, remote signals or barrier semaphores. Data moves between devices by JAX's collectives and lax.ppermute only.
A program may use at most 64 MiB of HBM per device.

v0:
```python
import functools
import math

import jax
import jax.numpy as jnp
from jax import lax
from jax.experimental import pallas as pl
from jax.experimental.pallas import tpu as pltpu
from jax.sharding import PartitionSpec as P


MOMENT = 0.95
COEF_ONE = 3.4445
COEF_THREE = -4.775
COEF_FIVE = 2.0315
SAFETY = 2.0
RATE = 0.5
SHRINK = 0.95


BF16 = jnp.bfloat16
F32 = jnp.float32


def swap(size, bit):
    return [(i, i ^ bit) for i in range(size)]


def shift(size, step):
    return [(i, (i + step) % size) for i in range(size)]


def dot(left, right):
    return jnp.dot(left, right, preferred_element_type=F32)


def unfold(size, place_ref, arrays, panel):
    rep = place_ref[2]
    fold = arrays[0].shape[1]
    nb = panel.shape[2]
    turn = (place_ref[1] + 1) * (fold // size)
    for array, side in ((arrays[0], rep), (arrays[1], 1 - rep)):
        for b in range(4):
            value = pltpu.roll(array[b].astype(F32), turn, 0).astype(BF16)
            for half in range(2):
                start = pl.multiple_of((2 * side + half) * fold, 16)
                panel[b, pl.ds(start, fold), :] = value[:, half * nb : (half + 1) * nb]


def chain_kernel(plan, size, tile, place_ref, *refs):
    count = len(refs) - 5
    arrays = refs[:count]
    out_ref, panel, buf, col, sem = refs[count:]
    n = buf.shape[1]
    nb = n // 4
    half = nb // 2
    edge = n // tile
    me = place_ref[0]
    row = place_ref[1]
    if plan is None:
        unfold(size, place_ref, arrays, panel)
    copies = []
    for index, (b, array, source, height, base, period, step) in enumerate(plan or ()):
        slot = lax.rem(row + (size - step), size)
        start = pl.multiple_of(base + slot * period, 16)
        copies.append(
            pltpu.make_async_copy(
                arrays[array].at[pl.ds(source, height), :],
                panel.at[b, pl.ds(start, height), :],
                sem.at[index],
            )
        )
    for copy in copies:
        copy.start()
    for copy in copies:
        copy.wait()

    bit_x = lax.rem(me, 2)
    bit_y = lax.div(me, 2)
    eye = lax.broadcasted_iota(jnp.int32, (tile, nb), 0) == lax.broadcasted_iota(
        jnp.int32, (tile, nb), 1
    )
    trace = jnp.zeros((1, 1), F32)
    for b in range(4):
        block = panel[b, 0:nb, :]
        buf[0, b * nb : (b + 1) * nb, b * nb : (b + 1) * nb] = block
        picked = jnp.where(eye[0:nb], block.astype(F32), 0.0)
        trace = trace + jnp.sum(picked, keepdims=True)
        own_x = bit_x ^ (b & 1)
        own_y = bit_y ^ (b >> 1)
        pairs = ((own_x, b ^ 1, b), (own_y, b ^ 2, b), (own_y, b ^ 2, b ^ 1))
        for index, (flag, high, low) in enumerate(pairs):
            part = panel[b, nb + index * half : nb + (index + 1) * half, :]
            tall = jnp.where(flag == 0, high, low)
            wide = jnp.where(flag == 0, low, high)
            rows = pl.multiple_of(tall * nb + flag * half, half)
            cols = pl.multiple_of(wide * nb, nb)
            buf[0, pl.ds(rows, half), pl.ds(cols, nb)] = part
            buf[0, pl.ds(cols, nb), pl.ds(rows, half)] = part.T

    def add_square(i, total):
        part = buf[0, pl.ds(pl.multiple_of(i * tile, tile), tile), :].astype(F32)
        return total + jnp.sum(part * part, keepdims=True)

    second = lax.fori_loop(0, edge, add_square, jnp.zeros((1, 1), F32))
    ratio = SAFETY * (second + 1.0) / (trace + 1.0)
    inverse = 1.0 / ratio
    scale = lax.rsqrt(ratio)
    one = jnp.ones((1, 1), F32)

    cells = [(i, j) for j in range(edge) for i in range(j, edge)]

    def product(step, carry):
        which = lax.div(step, len(cells))
        cell = lax.rem(step, len(cells))
        i = jnp.int32(0)
        j = jnp.int32(0)
        for index, (a, b) in enumerate(cells):
            i = jnp.where(cell == index, a, i)
            j = jnp.where(cell == index, b, j)
        square = (which == 0) | (which == 3)
        left = jnp.where(which == 2, 2, 0)
        right = jnp.where(square, 0, jnp.where(which == 4, 2, 1))
        into = jnp.where(
            which == 0, 1, jnp.where(which == 2, 0, jnp.where(which == 4, 3, 2))
        )
        linear = jnp.where(square, COEF_THREE, COEF_ONE) * jnp.where(which < 2, inverse, one)
        quad = jnp.where(square, COEF_FIVE, 1.0) * jnp.where(
            which == 0, inverse * inverse, jnp.where(which == 1, inverse, one)
        )
        rows = pl.ds(pl.multiple_of(i * tile, tile), tile)
        cols = pl.ds(pl.multiple_of(j * tile, tile), tile)
        acc = dot(buf[left, rows, :], buf[right, :, cols])
        value = (linear * buf[left, rows, cols].astype(F32) + quad * acc).astype(BF16)
        buf[into, rows, cols] = value

        @pl.when(i != j)
        def _():
            buf[into, cols, rows] = value.T

        return carry

    lax.fori_loop(0, 5 * len(cells), product, 0)

    unit = jnp.where(eye, 1.0, 0.0)
    col[0] = buf[2, :, 0:nb]
    col[0, 0:nb, :] = (buf[2, 0:nb, 0:nb].astype(F32) + COEF_ONE * unit[0:nb]).astype(BF16)
    col[2] = jnp.zeros((n, nb), BF16)

    def column(step, carry):
        which = lax.div(step, edge)
        i = lax.rem(step, edge)
        matrix = jnp.where((which == 0) | (which == 2), 3, 2)
        source = jnp.where(which == 1, 2, jnp.where(which == 2, 1, 0))
        into = jnp.where(which == 0, 2, jnp.where(which == 2, 0, 1))
        alpha = jnp.where((which == 0) | (which == 2), 0.0, COEF_ONE)
        beta = jnp.where(which == 2, COEF_FIVE, 1.0)
        gamma = jnp.where(which == 2, COEF_THREE, 0.0)
        delta = jnp.where((which == 2) & (i == 0), COEF_ONE, 0.0)
        rows = pl.ds(pl.multiple_of(i * tile, tile), tile)
        acc = dot(buf[matrix, rows, :], col[source])
        value = alpha * col[source, rows, :].astype(F32) + beta * acc
        value = value + gamma * col[2, rows, :].astype(F32) + delta * unit
        col[into, rows, :] = value.astype(BF16)
        return carry

    lax.fori_loop(0, 4 * edge, column, 0)

    def last(i, carry):
        rows = pl.ds(pl.multiple_of(i * tile, tile), tile)
        acc = dot(buf[1, rows, :], col[1])
        value = scale * (COEF_ONE * col[1, rows, :].astype(F32) + acc)
        out_ref[rows, :] = value.astype(BF16)
        return carry

    lax.fori_loop(0, edge, last, 0)


def chain(plan, arrays, place, size, n):
    nb = n // 4
    tile = min(n, 512)
    flops = int(5.0 * 2 * n**3)
    return pl.pallas_call(
        functools.partial(chain_kernel, plan, size, tile),
        out_shape=jax.ShapeDtypeStruct((n, nb), BF16),
        in_specs=[pl.BlockSpec(memory_space=pltpu.SMEM)]
        + [pl.BlockSpec(memory_space=pl.ANY if plan else pltpu.VMEM)] * len(arrays),
        out_specs=pl.BlockSpec(memory_space=pltpu.VMEM),
        scratch_shapes=[
            pltpu.VMEM((4, 5 * nb // 2, nb), BF16),
            pltpu.VMEM((4, n, n), BF16),
            pltpu.VMEM((3, n, nb), BF16),
            pltpu.SemaphoreType.DMA((len(plan or (0,)),)),
        ],
        compiler_params=pltpu.CompilerParams(
            vmem_limit_bytes=min(56, 8 + 24 * n * n // 2**20 // 2) * 2**20
        ),
        cost_estimate=pl.CostEstimate(flops=flops, bytes_accessed=6 * n * nb, transcendentals=0),
    )(place, *arrays)


def apply_kernel(a_ref, b_ref, c_ref, d_ref, q_ref, out_ref):
    nb = a_ref.shape[1]
    total = dot(a_ref[...], q_ref[0:nb, :])
    for index, ref in enumerate((b_ref, c_ref, d_ref)):
        total = total + dot(ref[...], q_ref[(index + 1) * nb : (index + 2) * nb, :])
    out_ref[...] = total.astype(BF16)


def apply(blocks, q):
    rows, nb = blocks[0].shape
    step = rows // 2 if rows % 32 == 0 else rows
    block = pl.BlockSpec((step, nb), lambda i: (i, 0))
    return pl.pallas_call(
        apply_kernel,
        grid=(rows // step,),
        in_specs=[block] * 4 + [pl.BlockSpec((4 * nb, nb), lambda i: (0, 0))],
        out_specs=block,
        out_shape=jax.ShapeDtypeStruct((rows, nb), BF16),
        compiler_params=pltpu.CompilerParams(vmem_limit_bytes=16 * 2**20),
        cost_estimate=pl.CostEstimate(
            flops=8 * rows * nb * nb, bytes_accessed=18 * rows * nb, transcendentals=0
        ),
    )(*blocks, q)


def own_kernel(*refs):
    out_ref = refs[-1]
    total = None
    for ref in refs[:-1]:
        value = ref[...]
        part = dot(value.T, value)
        total = part if total is None else total + part
    out_ref[...] = total.astype(BF16)


def own_gram(blocks):
    nb = blocks[0].shape[1]
    flops = sum(2 * block.shape[0] * nb * nb for block in blocks)
    return pl.pallas_call(
        own_kernel,
        out_shape=jax.ShapeDtypeStruct((nb, nb), BF16),
        compiler_params=pltpu.CompilerParams(vmem_limit_bytes=16 * 2**20),
        cost_estimate=pl.CostEstimate(flops=flops, bytes_accessed=2**20, transcendentals=0),
    )(*blocks)


def cross_kernel(count, place_ref, *refs):
    own, along_x, along_y = refs[0:count], refs[count : 2 * count], refs[2 * count : 3 * count]
    out_ref = refs[-1]
    half = out_ref.shape[1] // 2
    bit_x = lax.rem(place_ref[0], 2)
    bit_y = lax.div(place_ref[0], 2)

    def part(index, left, column, right):
        total = None
        for l_ref, r_ref in zip(left, right):
            value = dot(l_ref[:, column * half : (column + 1) * half].T, r_ref[...])
            total = value if total is None else total + value
        out_ref[index * half : (index + 1) * half, :] = total.astype(BF16)

    @pl.when(bit_x == 0)
    def _():
        part(0, along_x, 0, own)

    @pl.when(bit_x == 1)
    def _():
        part(0, own, 1, along_x)

    @pl.when(bit_y == 0)
    def _():
        part(1, along_y, 0, own)
        part(2, along_y, 0, along_x)

    @pl.when(bit_y == 1)
    def _():
        part(1, own, 1, along_y)
        part(2, along_x, 1, along_y)


def cross_gram(own, along_x, along_y, place):
    nb = own[0].shape[1]
    arrays = (*own, *along_x, *along_y)
    flops = sum(3 * block.shape[0] * nb * nb for block in own)
    return pl.pallas_call(
        functools.partial(cross_kernel, len(own)),
        out_shape=jax.ShapeDtypeStruct((3 * nb // 2, nb), BF16),
        in_specs=[pl.BlockSpec(memory_space=pltpu.SMEM)]
        + [pl.BlockSpec(memory_space=pltpu.VMEM)] * len(arrays),
        out_specs=pl.BlockSpec(memory_space=pltpu.VMEM),
        compiler_params=pltpu.CompilerParams(vmem_limit_bytes=24 * 2**20),
        cost_estimate=pl.CostEstimate(flops=flops, bytes_accessed=2**20, transcendentals=0),
    )(place, *arrays)


def scatter(chunk, size, place):
    return [
        lax.ppermute(chunk(lax.rem(place + step, size)), "fs", shift(size, step))
        for step in range(1, size)
    ]


def add_up(own, moved):
    total = own.astype(F32)
    for value in moved:
        total = total + value.astype(F32)
    return total.astype(BF16)


def spread(piece, size):
    return [lax.ppermute(piece, "fs", shift(size, step)) for step in range(1, size)]


def around(value):
    return [value] + [lax.ppermute(value, "tp", swap(4, b)) for b in (1, 2, 3)]


def pack_kernel(part, *refs):
    values = refs[:-2]
    out_ref = refs[-1]
    count = len(values)
    tail = values[0].shape[0] - part
    for index, ref in enumerate(values):
        out_ref[index * part : (index + 1) * part, :] = ref[0:part, :]
        if tail:
            start = count * part + (count - 1 - index) * tail
            out_ref[start : start + tail, :] = ref[part:, :]


def pack(values, later, part):
    rows = sum(value.shape[0] for value in values)
    return pl.pallas_call(
        functools.partial(pack_kernel, part),
        out_shape=jax.ShapeDtypeStruct((rows, values[0].shape[1]), BF16),
        in_specs=[pl.BlockSpec(memory_space=pltpu.VMEM)] * len(values)
        + [pl.BlockSpec(memory_space=pl.ANY)],
        out_specs=pl.BlockSpec(memory_space=pltpu.VMEM),
        compiler_params=pltpu.CompilerParams(vmem_limit_bytes=16 * 2**20),
    )(*values, later)


def relay(value, split):
    along_x = lax.ppermute(value, "tp", swap(4, 1))
    along_y = lax.ppermute(value, "tp", swap(4, 2))
    upper, lower = along_y[:split], along_x[split:]
    upper = lax.ppermute(upper, "tp", swap(4, 1))
    lower = lax.ppermute(lower, "tp", swap(4, 2))
    return [value, along_x, along_y, upper, lower]


def half_sum(grads, rep):
    height = grads.shape[1] // 2
    theirs = lax.dynamic_slice_in_dim(grads[0], (1 - rep) * height, height, 0)
    mine = lax.dynamic_slice_in_dim(grads[0], rep * height, height, 0)
    return mine, theirs.astype(BF16)


def local(f_size, *arrays):
    return update(f_size, *arrays)


def update(f_size, *arrays):
    rep = lax.axis_index("rep")
    tp = lax.axis_index("tp")
    fs = lax.axis_index("fs")
    place = jnp.stack([tp, fs, rep]).astype(jnp.int32)
    velocities = arrays[1::3]
    weights = arrays[2::3]
    heights = [arrays[3 * k].shape[1] * f_size for k in range(3)]
    cross = swap(2, 1)

    halves = [half_sum(arrays[3 * k], rep) for k in range(3)]
    received = [lax.ppermute(halves[k][1], "rep", cross) for k in range(3)]
    moments = [
        MOMENT * velocities[k] + (halves[k][0] + received[k].astype(F32)) for k in range(3)
    ]
    starts = [moment.astype(BF16) for moment in moments]
    small = starts[2]

    keep = jnp.where(rep == 0, starts[0], starts[1])
    give = jnp.where(rep == 0, starts[1], starts[0])
    small_x = lax.ppermute(small, "tp", swap(4, 1))
    small_y = lax.ppermute(small, "tp", swap(4, 2))
    small_d = lax.ppermute(small, "tp", swap(4, 3))
    keep_x = lax.ppermute(keep, "tp", swap(4, 1))
    keep_y = lax.ppermute(keep, "tp", swap(4, 2))
    gift = lax.ppermute(give, "rep", cross)
    gift_x = lax.ppermute(gift, "tp", swap(4, 1))
    gift_y = lax.ppermute(gift, "tp", swap(4, 2))

    small_panel = jnp.concatenate(
        [own_gram([small]), cross_gram([small], [small_x], [small_y], place)], axis=0
    )
    height = small_panel.shape[0] // 2
    fold = height // 2
    mine = lax.dynamic_slice_in_dim(small_panel, rep * height, height, 0)
    theirs = lax.dynamic_slice_in_dim(small_panel, (1 - rep) * height, height, 0)
    mine = mine.astype(F32) + lax.ppermute(theirs, "rep", cross).astype(F32)
    mine = mine.astype(BF16)
    mine = jnp.concatenate([mine[:fold], mine[fold:]], axis=1)
    diagonal = own_gram([keep, gift])
    nb = diagonal.shape[0]
    part = nb // f_size
    tail = fold // f_size

    def chunk(index):
        return jnp.concatenate(
            [
                lax.dynamic_slice_in_dim(diagonal, index * part, part, 0),
                lax.dynamic_slice_in_dim(mine, index * tail, tail, 0),
            ],
            axis=0,
        )

    total = add_up(chunk(fs), scatter(chunk, f_size, fs))
    parts = [total] + spread(total, f_size)
    rest = cross_gram([keep, gift], [keep_x, gift_x], [keep_y, gift_y], place)
    height = rest.shape[0] // f_size

    def slab(index):
        return lax.dynamic_slice_in_dim(rest, index * height, height, 0)

    moved = scatter(slab, f_size, fs)
    first_parts = pack(parts, rest, part)
    piece = add_up(slab(fs), moved)
    split = first_parts.shape[0] // 32 * 16
    first_groups = relay(first_parts, split)
    rest_parts = spread(piece, f_size)
    own_groups = around(piece)
    rest_parts = pack(rest_parts, piece, height)
    rest_groups = around(rest_parts)
    spreads = jnp.stack([group[nb:] for group in first_groups[:3]] + [first_groups[4][nb - split :]])
    others = lax.ppermute(spreads, "rep", cross)
    n = 4 * small.shape[1]
    small_q = chain(None, [spreads, others], place, f_size, n)
    small_out = apply([small, small_x, small_y, small_d], small_q)

    own_groups, rest_groups, first_groups, small_out, keep, gift = lax.optimization_barrier(
        (own_groups, rest_groups, first_groups, small_out, keep, gift)
    )
    n = 4 * nb
    plan = []
    for b in range(4):
        for step in range(f_size):
            low, high = step * part, (step + 1) * part
            if b < 3 or high <= split:
                plan.append((b, b, low, part, 0, part, step))
            elif low >= split:
                plan.append((b, 4, low - split, part, 0, part, step))
            else:
                plan.append((b, 3, low, split - low, 0, part, step))
                plan.append((b, 4, 0, high - split, split - low, part, step))
        plan.append((b, 5 + b, 0, height, nb, height, 0))
        for step in range(1, f_size):
            plan.append((b, 9 + b, (step - 1) * height, height, nb, height, step))
    both_q = chain(plan, [*first_groups, *own_groups, *rest_groups], place, f_size, n)

    gift_d = lax.ppermute(gift, "tp", swap(4, 3))
    keep_d = lax.ppermute(keep, "tp", swap(4, 3))
    sent = apply([gift, gift_x, gift_y, gift_d], both_q)
    arrived = lax.ppermute(sent, "rep", cross)
    kept = apply([keep, keep_x, keep_y, keep_d], both_q)
    finals = (
        jnp.where(rep == 0, kept, arrived),
        jnp.where(rep == 0, arrived, kept),
        small_out,
    )
    results = []
    for moment, final, weight, rows in zip(moments, finals, weights, heights):
        results.append(moment)
        results.append(SHRINK * weight - RATE * math.sqrt(rows) * final.astype(F32))
    return tuple(results)


def solution(mesh):
    grads = P("rep", "fs", "tp")
    state = P(("fs", "rep"), "tp")
    f_size = mesh.shape["fs"]
    return jax.shard_map(
        functools.partial(local, f_size),
        mesh=mesh,
        in_specs=(grads, state, state) * 3,
        out_specs=(state,) * 6,
        check_vma=False,
    )
```

profile of v0, /device:TPU:0, one launch (start us, length us, event | category | flops | bytes accessed | tf_op | source)
XLA Modules:
  0.0 278.9 jit_solution(18042011736388053217)
XLA Ops:
  0.6 2.4 fusion.2
  3.5 2.3 fusion.3
  5.8 1.1 fusion.7
  7.4 1.0 collective-permute-done.19
  8.4 1.7 fusion.12
  10.1 2.8 collective-permute-start.20
  12.9 1.5 collective-permute-start.21
  14.7 2.0 collective-permute-done.20.refs_1_.b_ref
  16.7 1.5 collective-permute-done.21.refs_2_.c_ref
  18.2 1.0 shard_map.140
  19.6 3.1 %broadcast_select_fusion = (bf16[704,512]{1,0:T(8,128)(2,1)S(1)}, f32[704,512]{1,0:T(8,128)S(1)}, f32[704,512]{1,0:T(8,128)S(1)}) fusion(pred[]{:T(512)S(6)} %eq.2, bf16[704,512]{1,0:T(8,128)(2,1)S(1)} %collective-permute-done.1, f32[1,1408,512]{2,1,0:T(8,128)} %param.12, s32[]{:T(128)S(6)} %select_n.76, f32[704,512]{1,0:T(8,128)S(1)} %copy-done.14, ...), kind=kLoop, calls=%fused_computation.10 | loop fusion | flops 3964928 | bytes 10813445 | tf_op jit(solution)/shard_map/jit(_where)/select_n | solution.py:381
  22.8 0.5 collective-permute-start.2
  24.3 0.8 collective-permute-done.2.refs_1_.a_ref
  25.1 1.0 shard_map.138
  26.2 1.6 collective-permute-start.23
  27.9 0.5 collective-permute-start.3
  28.4 1.5 collective-permute-start.5
  29.9 1.5 collective-permute-start.4
  31.9 2.9 %collective-permute-done.23 = bf16[168,512]{1,0:T(8,128)(2,1)S(1)} collective-permute-done((bf16[168,512]{1,0:T(8,128)(2,1)S(1)}, bf16[168,512]{1,0:T(8,128)(2,1)S(1)}, u32[]{:S(2)}, u32[]{:S(2)}) %collective-permute-start.23) | collective-permute-done | bytes 172064 | tf_op jit(solution)/shard_map/ppermute | solution.py:298
  34.8 0.7 collective-permute-start.24
  35.5 8.8 %collective-permute-done.24 = bf16[168,512]{1,0:T(8,128)(2,1)S(1)} collective-permute-done((bf16[168,512]{1,0:T(8,128)(2,1)S(1)}, bf16[168,512]{1,0:T(8,128)(2,1)S(1)}, u32[]{:S(2)}, u32[]{:S(2)}) %collective-permute-start.24) | collective-permute-done | bytes 172064 | tf_op jit(solution)/shard_map/ppermute | solution.py:298
  44.3 2.5 collective-permute-start.25
  46.8 4.1 %collective-permute-done.25 = bf16[168,512]{1,0:T(8,128)(2,1)S(1)} collective-permute-done((bf16[168,512]{1,0:T(8,128)(2,1)S(1)}, bf16[168,512]{1,0:T(8,128)(2,1)S(1)}, u32[]{:S(2)}, u32[]{:S(2)}) %collective-permute-start.25) | collective-permute-done | bytes 172064 | tf_op jit(solution)/shard_map/ppermute | solution.py:298
  51.1 4.8 %collective-permute-start.27 = (bf16[168,512]{1,0:T(8,128)(2,1)S(1)}, bf16[168,512]{1,0:T(8,128)(2,1)S(1)}, u32[]{:S(2)}, u32[]{:S(2)}) collective-permute-start(bf16[168,512]{1,0:T(8,128)(2,1)S(1)} %add_convert_fusion.1.refs_0_), channel_id=1, source_target_pairs={{0,16},{8,24},{16,0},{24,8},{1,17},{9,25},{17,1},{25,9},{2,18},{10... | collective-permute-start | bytes 516104 | tf_op jit(solution)/shard_map/ppermute | solution.py:311
  55.9 5.5 %collective-permute-done.4.refs_3_.b_ref = bf16[704,512]{1,0:T(8,128)(2,1)S(1)} collective-permute-done((bf16[704,512]{1,0:T(8,128)(2,1)S(1)}, bf16[704,512]{1,0:T(8,128)(2,1)S(1)}, u32[]{:S(2)}, u32[]{:S(2)}) %collective-permute-start.4) | collective-permute-done | bytes 720928 | tf_op jit(solution)/shard_map/ppermute | solution.py:388
  61.7 2.1 shard_map.136.refs_4_
  63.9 2.3 collective-permute-done.27.refs_2_
  66.2 0.9 shard_map.141.refs_0_
  67.1 0.5 collective-permute-start.29
  67.7 1.5 collective-permute-start.30
  69.2 0.8 constant_dynamic-slice_fusion.6
  70.0 4.2 %collective-permute-start.7 = (bf16[192,512]{1,0:T(8,128)(2,1)}, bf16[192,512]{1,0:T(8,128)(2,1)}, u32[]{:S(2)}, u32[]{:S(2)}) collective-permute-start(bf16[192,512]{1,0:T(8,128)(2,1)} %get-tuple-element.45), channel_id=1, source_target_pairs={{0,8},{8,16},{16,24},{24,0},{1,9},{9,17},{17,25},{25,1},{2,10},{10... | collective-permute-start | bytes 589832 | tf_op jit(solution)/shard_map/ppermute | solution.py:298
  74.1 2.3 collective-permute-start.9
  76.5 0.9 slice_bitcast_fusion.3
  77.4 7.3 %collective-permute-done.29.refs_1_ = bf16[672,512]{1,0:T(8,128)(2,1)} collective-permute-done((bf16[672,512]{1,0:T(8,128)(2,1)}, bf16[672,512]{1,0:T(8,128)(2,1)}, u32[]{:S(2)}, u32[]{:S(2)}) %collective-permute-start.29) | collective-permute-done | bytes 688160 | tf_op jit(solution)/shard_map/ppermute | solution.py:343
  84.7 1.0 slice.35
  85.7 1.6 collective-permute-start.32
  87.3 0.9 slice_bitcast_fusion.2
  88.2 0.9 slice_bitcast_fusion.1
  89.2 5.6 %collective-permute-done.32.refs_4_ = bf16[336,512]{1,0:T(8,128)(2,1)S(1)} collective-permute-done((bf16[336,512]{1,0:T(8,128)(2,1)S(1)}, bf16[336,512]{1,0:T(8,128)(2,1)S(1)}, u32[]{:S(2)}, u32[]{:S(2)}) %collective-permute-start.32) | collective-permute-done | bytes 344096 | tf_op jit(solution)/shard_map/ppermute | solution.py:347
  94.8 0.8 copy-done.17
  95.6 1.0 pad_maximum_fusion.refs_0_
  96.6 1.2 add_convert_fusion.refs_3_.refs_5_
  97.8 4.4 %collective-permute-start.13 = (bf16[192,512]{1,0:T(8,128)(2,1)S(1)}, bf16[192,512]{1,0:T(8,128)(2,1)S(1)}, u32[]{:S(2)}, u32[]{:S(2)}) collective-permute-start(bf16[192,512]{1,0:T(8,128)(2,1)S(1)} %add_convert_fusion.refs_3_.refs_5_), channel_id=1, source_target_pairs={{0,8},{8,16},{16,24},{24,0},{1,9},{9,17},{17,25},{25,1},{2,10},{10... | collective-permute-start | bytes 589832 | tf_op jit(solution)/shard_map/ppermute | solution.py:311
  102.2 2.4 collective-permute-start.15
  105.2 2.4 collective-permute-done.13.refs_0_
  107.5 1.5 collective-permute-start.11
  109.0 6.4 %collective-permute-done.14.refs_1_ = bf16[192,512]{1,0:T(8,128)(2,1)S(1)} collective-permute-done((bf16[192,512]{1,0:T(8,128)(2,1)S(1)}, bf16[192,512]{1,0:T(8,128)(2,1)S(1)}, u32[]{:S(2)}, u32[]{:S(2)}) %collective-permute-start.14) | collective-permute-done | bytes 196640 | tf_op jit(solution)/shard_map/ppermute | solution.py:311
  115.4 1.5 collective-permute-start.33
  116.9 1.4 collective-permute-start.12
  118.4 1.2 slice.34
  119.6 3.1 %collective-permute-done.33.d_ref = bf16[256,256]{1,0:T(8,128)(2,1)S(1)} collective-permute-done((bf16[256,256]{1,0:T(8,128)(2,1)S(1)}, bf16[256,256]{1,0:T(8,128)(2,1)S(1)}, u32[]{:S(2)}, u32[]{:S(2)}) %collective-permute-start.33) | collective-permute-done | bytes 131104 | tf_op jit(solution)/shard_map/ppermute | solution.py:384
  122.9 1.9 collective-permute-start.17
  124.8 1.4 collective-permute-start.18
  126.4 21.6 %shard_map.142.q_ref = bf16[1024,256]{1,0:T(8,128)(2,1)S(1)} custom-call(s32[3]{0:T(128)S(1)} %pad_add_fusion.place_ref, bf16[4,160,512]{2,1,0:T(8,128)(2,1)} %pad_maximum_fusion.refs_0_, bf16[4,160,512]{2,1,0:T(8,128)(2,1)} %collective-permute-done.34.refs_1_), custom_call_target="tpu_custom_call" | custom-call | flops 10737418240 | bytes 1572864 | tf_op jit(solution)/shard_map/pallas_call | solution.py:183
  148.6 3.9 %collective-permute-done.18.refs_12_ = bf16[576,512]{1,0:T(8,128)(2,1)S(1)} collective-permute-done((bf16[576,512]{1,0:T(8,128)(2,1)S(1)}, bf16[576,512]{1,0:T(8,128)(2,1)S(1)}, u32[]{:S(2)}, u32[]{:S(2)}) %collective-permute-start.18) | collective-permute-done | bytes 589856 | tf_op jit(solution)/shard_map/ppermute | solution.py:315
  152.5 6.1 %collective-permute-done.31.refs_3_ = bf16[336,512]{1,0:T(8,128)(2,1)S(1)} collective-permute-done((bf16[336,512]{1,0:T(8,128)(2,1)S(1)}, bf16[336,512]{1,0:T(8,128)(2,1)S(1)}, u32[]{:S(2)}, u32[]{:S(2)}) %collective-permute-start.31) | collective-permute-done | bytes 344096 | tf_op jit(solution)/shard_map/ppermute | solution.py:346
  159.1 2.5 collective-permute-start.36
  161.6 109.0 %shard_map.144.q_ref = bf16[2048,512]{1,0:T(8,128)(2,1)} custom-call(s32[3]{0:T(128)} %copy-done.9, bf16[672,512]{1,0:T(8,128)(2,1)} %shard_map.141.refs_0_, bf16[672,512]{1,0:T(8,128)(2,1)} %collective-permute-done.29.refs_1_, bf16[672,512]{1,0:T(8,128)(2,1)} %collective-permute-done.30.refs_2_, bf16[336,512]{1,0:T(8,128)(2,1)} %copy-done.21, ...), custom_call_target="tpu_custom_call" | custom-call | flops 85899345920 | bytes 6291456 | tf_op jit(solution)/shard_map/pallas_call | solution.py:183
  270.7 1.6 copy-done
  272.2 1.8 shard_map.146
  274.2 0.7 multiply_subtract_fusion.2
  274.9 1.8 shard_map.145
  276.8 2.1 multiply_subtract_fusion
  (100 shorter events, 5.8 us)
Async XLA Ops:
  0.6 7.8 %copy-start.16 = (f32[256,256]{1,0:T(8,128)S(1)}, f32[256,256]{1,0:T(8,128)}, u32[]{:S(2)}) copy-start(f32[256,256]{1,0:T(8,128)} %param.16) | copy-start | bytes 786436
  3.0 16.6 %collective-permute-start = (bf16[704,512]{1,0:T(8,128)(2,1)}, bf16[704,512]{1,0:T(8,128)(2,1)S(1)}, u32[]{:S(2)}, u32[]{:S(2)}) collective-permute-start(bf16[704,512]{1,0:T(8,128)(2,1)} %fusion.2), channel_id=1, source_target_pairs={{0,1},{1,0},{2,3},{3,2},{4,5},{5,4},{6,7},{7,6},{8,9},{9,8},{10,11... | collective-permute-start | bytes 2162696 | tf_op jit(solution)/shard_map/ppermute | solution.py:373
  5.8 13.8 %copy-start.14 = (f32[704,512]{1,0:T(8,128)S(1)}, f32[704,512]{1,0:T(8,128)}, u32[]{:S(2)}) copy-start(f32[704,512]{1,0:T(8,128)} %param.13) | copy-start | bytes 4325380
  5.8 13.8 %collective-permute-start.1 = (bf16[704,512]{1,0:T(8,128)(2,1)}, bf16[704,512]{1,0:T(8,128)(2,1)S(1)}, u32[]{:S(2)}, u32[]{:S(2)}) collective-permute-start(bf16[704,512]{1,0:T(8,128)(2,1)} %fusion.3), channel_id=1, source_target_pairs={{0,1},{1,0},{2,3},{3,2},{4,5},{5,4},{6,7},{7,6},{8,9},{9,8},{10,11... | collective-permute-start | bytes 2162696 | tf_op jit(solution)/shard_map/ppermute | solution.py:373
  6.9 1.5 collective-permute-start.19
  10.1 6.6 %collective-permute-start.20 = (bf16[256,256]{1,0:T(8,128)(2,1)S(1)}, bf16[256,256]{1,0:T(8,128)(2,1)S(1)}, u32[]{:S(2)}, u32[]{:S(2)}) collective-permute-start(bf16[256,256]{1,0:T(8,128)(2,1)S(1)} %get-tuple-element.38.refs_0_.a_ref), channel_id=1, source_target_pairs={{0,2},{2,0},{4,6},{6,4},{1,3},{3,1},{5,7},{7,5},{8,10},{10,8},{12,... | collective-permute-start | bytes 393224 | tf_op jit(solution)/shard_map/ppermute | solution.py:382
  12.9 5.3 %collective-permute-start.21 = (bf16[256,256]{1,0:T(8,128)(2,1)S(1)}, bf16[256,256]{1,0:T(8,128)(2,1)S(1)}, u32[]{:S(2)}, u32[]{:S(2)}) collective-permute-start(bf16[256,256]{1,0:T(8,128)(2,1)S(1)} %get-tuple-element.38.refs_0_.a_ref), channel_id=1, source_target_pairs={{0,4},{2,6},{4,0},{6,2},{1,5},{3,7},{5,1},{7,3},{8,12},{10,14},{12... | collective-permute-start | bytes 393224 | tf_op jit(solution)/shard_map/ppermute | solution.py:383
  14.5 111.9 %copy-start.9 = (s32[3]{0:T(128)}, s32[3]{0:T(128)S(1)}, u32[]{:S(2)}) copy-start(s32[3]{0:T(128)S(1)} %pad_add_fusion.place_ref) | copy-start | bytes 40
  19.5 3.8 %collective-permute-start.22 = (bf16[320,256]{1,0:T(8,128)(2,1)S(1)}, bf16[320,256]{1,0:T(8,128)(2,1)S(1)}, u32[]{:S(2)}, u32[]{:S(2)}) collective-permute-start(bf16[320,256]{1,0:T(8,128)(2,1)S(1)} %fusion.5), channel_id=1, source_target_pairs={{0,1},{1,0},{2,3},{3,2},{4,5},{5,4},{6,7},{7,6},{8,9},{9,8},{10,11... | collective-permute-start | bytes 491528 | tf_op jit(solution)/shard_map/ppermute | solution.py:398
  22.8 1.3 copy-start.10
  22.8 1.6 copy-start.11
  22.8 2.4 collective-permute-start.2
  26.2 8.6 %collective-permute-start.23 = (bf16[168,512]{1,0:T(8,128)(2,1)S(1)}, bf16[168,512]{1,0:T(8,128)(2,1)S(1)}, u32[]{:S(2)}, u32[]{:S(2)}) collective-permute-start(bf16[168,512]{1,0:T(8,128)(2,1)S(1)} %pad_maximum_fusion.1), channel_id=1, source_target_pairs={{0,8},{8,16},{16,24},{24,0},{1,9},{9,17},{17,25},{25,1},{2,10},{10... | collective-permute-start | bytes 516104 | tf_op jit(solution)/shard_map/ppermute | solution.py:298
  27.9 23.2 %collective-permute-start.3 = (bf16[704,512]{1,0:T(8,128)(2,1)S(1)}, bf16[704,512]{1,0:T(8,128)(2,1)S(1)}, u32[]{:S(2)}, u32[]{:S(2)}) collective-permute-start(bf16[704,512]{1,0:T(8,128)(2,1)S(1)} %broadcast_select_fusion.1.refs_0_.a_ref), channel_id=1, source_target_pairs={{0,2},{2,0},{4,6},{6,4},{1,3},{3,1},{5,7},{7,5},{8,10},{10,8},{12,... | collective-permute-start | bytes 2162696 | tf_op jit(solution)/shard_map/ppermute | solution.py:385
  28.4 27.5 %collective-permute-start.5 = (bf16[704,512]{1,0:T(8,128)(2,1)S(1)}, bf16[704,512]{1,0:T(8,128)(2,1)S(1)}, u32[]{:S(2)}, u32[]{:S(2)}) collective-permute-start(bf16[704,512]{1,0:T(8,128)(2,1)S(1)} %broadcast_select_fusion.1.refs_0_.a_ref), channel_id=1, source_target_pairs={{0,4},{2,6},{4,0},{6,2},{1,5},{3,7},{5,1},{7,3},{8,12},{10,14},{12... | collective-permute-start | bytes 2162696 | tf_op jit(solution)/shard_map/ppermute | solution.py:386
  29.9 31.5 %collective-permute-start.4 = (bf16[704,512]{1,0:T(8,128)(2,1)S(1)}, bf16[704,512]{1,0:T(8,128)(2,1)S(1)}, u32[]{:S(2)}, u32[]{:S(2)}) collective-permute-start(bf16[704,512]{1,0:T(8,128)(2,1)S(1)} %collective-permute-done.2.refs_1_.a_ref), channel_id=1, source_target_pairs={{0,2},{2,0},{4,6},{6,4},{1,3},{3,1},{5,7},{7,5},{8,10},{10,8},{12,... | collective-permute-start | bytes 2162696 | tf_op jit(solution)/shard_map/ppermute | solution.py:388
  31.4 30.3 %collective-permute-start.6 = (bf16[704,512]{1,0:T(8,128)(2,1)S(1)}, bf16[704,512]{1,0:T(8,128)(2,1)S(1)}, u32[]{:S(2)}, u32[]{:S(2)}) collective-permute-start(bf16[704,512]{1,0:T(8,128)(2,1)S(1)} %collective-permute-done.2.refs_1_.a_ref), channel_id=1, source_target_pairs={{0,4},{2,6},{4,0},{6,2},{1,5},{3,7},{5,1},{7,3},{8,12},{10,14},{12... | collective-permute-start | bytes 2162696 | tf_op jit(solution)/shard_map/ppermute | solution.py:389
  34.8 9.5 %collective-permute-start.24 = (bf16[168,512]{1,0:T(8,128)(2,1)S(1)}, bf16[168,512]{1,0:T(8,128)(2,1)S(1)}, u32[]{:S(2)}, u32[]{:S(2)}) collective-permute-start(bf16[168,512]{1,0:T(8,128)(2,1)S(1)} %pad_maximum_fusion.2), channel_id=1, source_target_pairs={{0,16},{8,24},{16,0},{24,8},{1,17},{9,25},{17,1},{25,9},{2,18},{10... | collective-permute-start | bytes 516104 | tf_op jit(solution)/shard_map/ppermute | solution.py:298
  44.3 6.6 %collective-permute-start.25 = (bf16[168,512]{1,0:T(8,128)(2,1)S(1)}, bf16[168,512]{1,0:T(8,128)(2,1)S(1)}, u32[]{:S(2)}, u32[]{:S(2)}) collective-permute-start(bf16[168,512]{1,0:T(8,128)(2,1)S(1)} %pad_maximum_fusion.3), channel_id=1, source_target_pairs={{0,24},{8,0},{16,8},{24,16},{1,25},{9,1},{17,9},{25,17},{2,26},{10... | collective-permute-start | bytes 516104 | tf_op jit(solution)/shard_map/ppermute | solution.py:298
  51.0 12.9 %collective-permute-start.26 = (bf16[168,512]{1,0:T(8,128)(2,1)S(1)}, bf16[168,512]{1,0:T(8,128)(2,1)S(1)}, u32[]{:S(2)}, u32[]{:S(2)}) collective-permute-start(bf16[168,512]{1,0:T(8,128)(2,1)S(1)} %add_convert_fusion.1.refs_0_), channel_id=1, source_target_pairs={{0,8},{8,16},{16,24},{24,0},{1,9},{9,17},{17,25},{25,1},{2,10},{10... | collective-permute-start | bytes 516104 | tf_op jit(solution)/shard_map/ppermute | solution.py:311
  51.1 15.1 %collective-permute-start.27 = (bf16[168,512]{1,0:T(8,128)(2,1)S(1)}, bf16[168,512]{1,0:T(8,128)(2,1)S(1)}, u32[]{:S(2)}, u32[]{:S(2)}) collective-permute-start(bf16[168,512]{1,0:T(8,128)(2,1)S(1)} %add_convert_fusion.1.refs_0_), channel_id=1, source_target_pairs={{0,16},{8,24},{16,0},{24,8},{1,17},{9,25},{17,1},{25,9},{2,18},{10... | collective-permute-start | bytes 516104 | tf_op jit(solution)/shard_map/ppermute | solution.py:311
  55.9 8.0 %copy-start.1 = (bf16[704,512]{1,0:T(8,128)(2,1)}, bf16[704,512]{1,0:T(8,128)(2,1)S(1)}, u32[]{:S(2)}) copy-start(bf16[704,512]{1,0:T(8,128)(2,1)S(1)} %collective-permute-done.5.refs_4_.c_ref) | copy-start | bytes 2162692
  55.9 10.3 %collective-permute-start.28 = (bf16[168,512]{1,0:T(8,128)(2,1)S(1)}, bf16[168,512]{1,0:T(8,128)(2,1)S(1)}, u32[]{:S(2)}, u32[]{:S(2)}) collective-permute-start(bf16[168,512]{1,0:T(8,128)(2,1)S(1)} %add_convert_fusion.1.refs_0_), channel_id=1, source_target_pairs={{0,24},{8,0},{16,8},{24,16},{1,25},{9,1},{17,9},{25,17},{2,26},{10... | collective-permute-start | bytes 516104 | tf_op jit(solution)/shard_map/ppermute | solution.py:311
  61.4 2.4 copy-start.3
  61.7 2.2 copy-start.5
  67.1 17.6 %collective-permute-start.29 = (bf16[672,512]{1,0:T(8,128)(2,1)}, bf16[672,512]{1,0:T(8,128)(2,1)}, u32[]{:S(2)}, u32[]{:S(2)}) collective-permute-start(bf16[672,512]{1,0:T(8,128)(2,1)} %shard_map.141.refs_0_), channel_id=1, source_target_pairs={{0,2},{2,0},{4,6},{6,4},{1,3},{3,1},{5,7},{7,5},{8,10},{10,8},{12,... | collective-permute-start | bytes 2064392 | tf_op jit(solution)/shard_map/ppermute | solution.py:343
  67.7 20.6 %collective-permute-start.30 = (bf16[672,512]{1,0:T(8,128)(2,1)}, bf16[672,512]{1,0:T(8,128)(2,1)}, u32[]{:S(2)}, u32[]{:S(2)}) collective-permute-start(bf16[672,512]{1,0:T(8,128)(2,1)} %shard_map.141.refs_0_), channel_id=1, source_target_pairs={{0,4},{2,6},{4,0},{6,2},{1,5},{3,7},{5,1},{7,3},{8,12},{10,14},{12... | collective-permute-start | bytes 2064392 | tf_op jit(solution)/shard_map/ppermute | solution.py:344
  70.0 26.6 %collective-permute-start.7 = (bf16[192,512]{1,0:T(8,128)(2,1)}, bf16[192,512]{1,0:T(8,128)(2,1)}, u32[]{:S(2)}, u32[]{:S(2)}) collective-permute-start(bf16[192,512]{1,0:T(8,128)(2,1)} %get-tuple-element.45), channel_id=1, source_target_pairs={{0,8},{8,16},{16,24},{24,0},{1,9},{9,17},{17,25},{25,1},{2,10},{10... | collective-permute-start | bytes 589832 | tf_op jit(solution)/shard_map/ppermute | solution.py:298
  74.1 22.4 %collective-permute-start.8 = (bf16[192,512]{1,0:T(8,128)(2,1)}, bf16[192,512]{1,0:T(8,128)(2,1)}, u32[]{:S(2)}, u32[]{:S(2)}) collective-permute-start(bf16[192,512]{1,0:T(8,128)(2,1)} %get-tuple-element.47), channel_id=1, source_target_pairs={{0,16},{8,24},{16,0},{24,8},{1,17},{9,25},{17,1},{25,9},{2,18},{10... | collective-permute-start | bytes 589832 | tf_op jit(solution)/shard_map/ppermute | solution.py:298
  74.1 22.4 %collective-permute-start.9 = (bf16[192,512]{1,0:T(8,128)(2,1)S(1)}, bf16[192,512]{1,0:T(8,128)(2,1)}, u32[]{:S(2)}, u32[]{:S(2)}) collective-permute-start(bf16[192,512]{1,0:T(8,128)(2,1)S(1)} %get-tuple-element.46), channel_id=1, source_target_pairs={{0,24},{8,0},{16,8},{24,16},{1,25},{9,1},{17,9},{25,17},{2,26},{10... | collective-permute-start | bytes 589832 | tf_op jit(solution)/shard_map/ppermute | solution.py:298
  85.7 9.1 %collective-permute-start.32 = (bf16[336,512]{1,0:T(8,128)(2,1)S(1)}, bf16[336,512]{1,0:T(8,128)(2,1)S(1)}, u32[]{:S(2)}, u32[]{:S(2)}) collective-permute-start(bf16[336,512]{1,0:T(8,128)(2,1)S(1)} %slice.35), channel_id=1, source_target_pairs={{0,4},{2,6},{4,0},{6,2},{1,5},{3,7},{5,1},{7,3},{8,12},{10,14},{12... | collective-permute-start | bytes 1032200 | tf_op jit(solution)/shard_map/ppermute | solution.py:347
  94.8 0.8 copy-start.17
  96.5 29.7 %collective-permute-start.34 = (bf16[4,160,512]{2,1,0:T(8,128)(2,1)}, bf16[4,160,512]{2,1,0:T(8,128)(2,1)}, u32[]{:S(2)}, u32[]{:S(2)}) collective-permute-start(bf16[4,160,512]{2,1,0:T(8,128)(2,1)} %pad_maximum_fusion.refs_0_), channel_id=1, source_target_pairs={{0,1},{1,0},{2,3},{3,2},{4,5},{5,4},{6,7},{7,6},{8,9},{9,8},{10,11... | collective-permute-start | bytes 1966088 | tf_op jit(solution)/shard_map/ppermute | solution.py:433
  97.8 50.2 %copy-start.7 = (bf16[192,512]{1,0:T(8,128)(2,1)}, bf16[192,512]{1,0:T(8,128)(2,1)S(1)}, u32[]{:S(2)}) copy-start(bf16[192,512]{1,0:T(8,128)(2,1)S(1)} %add_convert_fusion.refs_3_.refs_5_) | copy-start | bytes 589828
  97.8 9.7 %collective-permute-start.13 = (bf16[192,512]{1,0:T(8,128)(2,1)S(1)}, bf16[192,512]{1,0:T(8,128)(2,1)S(1)}, u32[]{:S(2)}, u32[]{:S(2)}) collective-permute-start(bf16[192,512]{1,0:T(8,128)(2,1)S(1)} %add_convert_fusion.refs_3_.refs_5_), channel_id=1, source_target_pairs={{0,8},{8,16},{16,24},{24,0},{1,9},{9,17},{17,25},{25,1},{2,10},{10... | collective-permute-start | bytes 589832 | tf_op jit(solution)/shard_map/ppermute | solution.py:311
  102.2 13.3 %collective-permute-start.14 = (bf16[192,512]{1,0:T(8,128)(2,1)S(1)}, bf16[192,512]{1,0:T(8,128)(2,1)S(1)}, u32[]{:S(2)}, u32[]{:S(2)}) collective-permute-start(bf16[192,512]{1,0:T(8,128)(2,1)S(1)} %add_convert_fusion.refs_3_.refs_5_), channel_id=1, source_target_pairs={{0,16},{8,24},{16,0},{24,8},{1,17},{9,25},{17,1},{25,9},{2,18},{10... | collective-permute-start | bytes 589832 | tf_op jit(solution)/shard_map/ppermute | solution.py:311
  102.2 14.8 %collective-permute-start.15 = (bf16[192,512]{1,0:T(8,128)(2,1)S(1)}, bf16[192,512]{1,0:T(8,128)(2,1)S(1)}, u32[]{:S(2)}, u32[]{:S(2)}) collective-permute-start(bf16[192,512]{1,0:T(8,128)(2,1)S(1)} %add_convert_fusion.refs_3_.refs_5_), channel_id=1, source_target_pairs={{0,24},{8,0},{16,8},{24,16},{1,25},{9,1},{17,9},{25,17},{2,26},{10... | collective-permute-start | bytes 589832 | tf_op jit(solution)/shard_map/ppermute | solution.py:311
  104.6 18.3 %collective-permute-start.10 = (bf16[192,512]{1,0:T(8,128)(2,1)S(1)}, bf16[192,512]{1,0:T(8,128)(2,1)S(1)}, u32[]{:S(2)}, u32[]{:S(2)}) collective-permute-start(bf16[192,512]{1,0:T(8,128)(2,1)S(1)} %add_convert_fusion.refs_3_.refs_5_), channel_id=1, source_target_pairs={{0,2},{2,0},{4,6},{6,4},{1,3},{3,1},{5,7},{7,5},{8,10},{10,8},{12,... | collective-permute-start | bytes 589832 | tf_op jit(solution)/shard_map/ppermute | solution.py:315
  107.5 17.3 %collective-permute-start.11 = (bf16[192,512]{1,0:T(8,128)(2,1)S(1)}, bf16[192,512]{1,0:T(8,128)(2,1)S(1)}, u32[]{:S(2)}, u32[]{:S(2)}) collective-permute-start(bf16[192,512]{1,0:T(8,128)(2,1)S(1)} %add_convert_fusion.refs_3_.refs_5_), channel_id=1, source_target_pairs={{0,4},{2,6},{4,0},{6,2},{1,5},{3,7},{5,1},{7,3},{8,12},{10,14},{12... | collective-permute-start | bytes 589832 | tf_op jit(solution)/shard_map/ppermute | solution.py:315
  115.4 7.3 %collective-permute-start.33 = (bf16[256,256]{1,0:T(8,128)(2,1)S(1)}, bf16[256,256]{1,0:T(8,128)(2,1)S(1)}, u32[]{:S(2)}, u32[]{:S(2)}) collective-permute-start(bf16[256,256]{1,0:T(8,128)(2,1)S(1)} %get-tuple-element.38.refs_0_.a_ref), channel_id=1, source_target_pairs={{0,6},{2,4},{4,2},{6,0},{1,7},{3,5},{5,3},{7,1},{8,14},{10,12},{12... | collective-permute-start | bytes 393224 | tf_op jit(solution)/shard_map/ppermute | solution.py:384
  116.9 31.6 %collective-permute-start.12 = (bf16[192,512]{1,0:T(8,128)(2,1)S(1)}, bf16[192,512]{1,0:T(8,128)(2,1)S(1)}, u32[]{:S(2)}, u32[]{:S(2)}) collective-permute-start(bf16[192,512]{1,0:T(8,128)(2,1)S(1)} %add_convert_fusion.refs_3_.refs_5_), channel_id=1, source_target_pairs={{0,6},{2,4},{4,2},{6,0},{1,7},{3,5},{5,3},{7,1},{8,14},{10,12},{12... | collective-permute-start | bytes 589832 | tf_op jit(solution)/shard_map/ppermute | solution.py:315
  118.4 29.6 %copy-start.8 = (bf16[576,512]{1,0:T(8,128)(2,1)}, bf16[576,512]{1,0:T(8,128)(2,1)S(1)}, u32[]{:S(2)}) copy-start(bf16[576,512]{1,0:T(8,128)(2,1)S(1)} %shard_map.137.refs_9_) | copy-start | bytes 1769476
  122.7 25.9 %collective-permute-start.16 = (bf16[576,512]{1,0:T(8,128)(2,1)S(1)}, bf16[576,512]{1,0:T(8,128)(2,1)S(1)}, u32[]{:S(2)}, u32[]{:S(2)}) collective-permute-start(bf16[576,512]{1,0:T(8,128)(2,1)S(1)} %shard_map.137.refs_9_), channel_id=1, source_target_pairs={{0,2},{2,0},{4,6},{6,4},{1,3},{3,1},{5,7},{7,5},{8,10},{10,8},{12,... | collective-permute-start | bytes 1769480 | tf_op jit(solution)/shard_map/ppermute | solution.py:315
  122.9 25.1 %copy-start.22 = (bf16[192,512]{1,0:T(8,128)(2,1)}, bf16[192,512]{1,0:T(8,128)(2,1)S(1)}, u32[]{:S(2)}) copy-start(bf16[192,512]{1,0:T(8,128)(2,1)S(1)} %collective-permute-done.10.refs_6_) | copy-start | bytes 589828
  122.9 25.7 %collective-permute-start.17 = (bf16[576,512]{1,0:T(8,128)(2,1)S(1)}, bf16[576,512]{1,0:T(8,128)(2,1)S(1)}, u32[]{:S(2)}, u32[]{:S(2)}) collective-permute-start(bf16[576,512]{1,0:T(8,128)(2,1)S(1)} %shard_map.137.refs_9_), channel_id=1, source_target_pairs={{0,4},{2,6},{4,0},{6,2},{1,5},{3,7},{5,1},{7,3},{8,12},{10,14},{12... | collective-permute-start | bytes 1769480 | tf_op jit(solution)/shard_map/ppermute | solution.py:315
  124.8 23.2 %copy-start.23 = (bf16[192,512]{1,0:T(8,128)(2,1)}, bf16[192,512]{1,0:T(8,128)(2,1)S(1)}, u32[]{:S(2)}) copy-start(bf16[192,512]{1,0:T(8,128)(2,1)S(1)} %collective-permute-done.11.refs_7_) | copy-start | bytes 589828
  124.8 27.7 %collective-permute-start.18 = (bf16[576,512]{1,0:T(8,128)(2,1)S(1)}, bf16[576,512]{1,0:T(8,128)(2,1)S(1)}, u32[]{:S(2)}, u32[]{:S(2)}) collective-permute-start(bf16[576,512]{1,0:T(8,128)(2,1)S(1)} %shard_map.137.refs_9_), channel_id=1, source_target_pairs={{0,6},{2,4},{4,2},{6,0},{1,7},{3,5},{5,3},{7,1},{8,14},{10,12},{12... | collective-permute-start | bytes 1769480 | tf_op jit(solution)/shard_map/ppermute | solution.py:315
  126.2 32.4 %collective-permute-start.31 = (bf16[336,512]{1,0:T(8,128)(2,1)S(1)}, bf16[336,512]{1,0:T(8,128)(2,1)S(1)}, u32[]{:S(2)}, u32[]{:S(2)}) collective-permute-start(bf16[336,512]{1,0:T(8,128)(2,1)S(1)} %slice.34), channel_id=1, source_target_pairs={{0,2},{2,0},{4,6},{6,4},{1,3},{3,1},{5,7},{7,5},{8,10},{10,8},{12,... | collective-permute-start | bytes 1032200 | tf_op jit(solution)/shard_map/ppermute | solution.py:346
  148.5 122.1 %copy-start.4 = (bf16[704,512]{1,0:T(8,128)(2,1)S(1)}, bf16[704,512]{1,0:T(8,128)(2,1)}, u32[]{:S(2)}) copy-start(bf16[704,512]{1,0:T(8,128)(2,1)} %copy-done.3) | copy-start | bytes 2162692
  148.5 122.1 %copy-start.6 = (bf16[704,512]{1,0:T(8,128)(2,1)S(1)}, bf16[704,512]{1,0:T(8,128)(2,1)}, u32[]{:S(2)}) copy-start(bf16[704,512]{1,0:T(8,128)(2,1)} %copy-done.5) | copy-start | bytes 2162692
  148.6 4.0 %copy-start.24 = (bf16[192,512]{1,0:T(8,128)(2,1)}, bf16[192,512]{1,0:T(8,128)(2,1)S(1)}, u32[]{:S(2)}) copy-start(bf16[192,512]{1,0:T(8,128)(2,1)S(1)} %collective-permute-done.12.refs_8_) | copy-start | bytes 589828
  148.6 13.0 %copy-start.18 = (bf16[576,512]{1,0:T(8,128)(2,1)}, bf16[576,512]{1,0:T(8,128)(2,1)S(1)}, u32[]{:S(2)}) copy-start(bf16[576,512]{1,0:T(8,128)(2,1)S(1)} %collective-permute-done.16.refs_10_) | copy-start | bytes 1769476
  148.6 13.0 %copy-start.19 = (bf16[576,512]{1,0:T(8,128)(2,1)}, bf16[576,512]{1,0:T(8,128)(2,1)S(1)}, u32[]{:S(2)}) copy-start(bf16[576,512]{1,0:T(8,128)(2,1)S(1)} %collective-permute-done.17.refs_11_) | copy-start | bytes 1769476
  152.5 9.1 %copy-start.20 = (bf16[576,512]{1,0:T(8,128)(2,1)}, bf16[576,512]{1,0:T(8,128)(2,1)S(1)}, u32[]{:S(2)}) copy-start(bf16[576,512]{1,0:T(8,128)(2,1)S(1)} %collective-permute-done.18.refs_12_) | copy-start | bytes 1769476
  158.7 2.9 %copy-start.21 = (bf16[336,512]{1,0:T(8,128)(2,1)}, bf16[336,512]{1,0:T(8,128)(2,1)S(1)}, u32[]{:S(2)}) copy-start(bf16[336,512]{1,0:T(8,128)(2,1)S(1)} %collective-permute-done.31.refs_3_) | copy-start | bytes 1032196
  158.7 116.3 %collective-permute-start.35 = (bf16[704,512]{1,0:T(8,128)(2,1)S(1)}, bf16[704,512]{1,0:T(8,128)(2,1)S(1)}, u32[]{:S(2)}, u32[]{:S(2)}) collective-permute-start(bf16[704,512]{1,0:T(8,128)(2,1)S(1)} %broadcast_select_fusion.1.refs_0_.a_ref), channel_id=1, source_target_pairs={{0,6},{2,4},{4,2},{6,0},{1,7},{3,5},{5,3},{7,1},{8,14},{10,12},{12... | collective-permute-start | bytes 2162696 | tf_op jit(solution)/shard_map/ppermute | solution.py:459
  159.1 111.5 %collective-permute-start.36 = (bf16[704,512]{1,0:T(8,128)(2,1)S(1)}, bf16[704,512]{1,0:T(8,128)(2,1)S(1)}, u32[]{:S(2)}, u32[]{:S(2)}) collective-permute-start(bf16[704,512]{1,0:T(8,128)(2,1)S(1)} %collective-permute-done.2.refs_1_.a_ref), channel_id=1, source_target_pairs={{0,6},{2,4},{4,2},{6,0},{1,7},{3,5},{5,3},{7,1},{8,14},{10,12},{12... | collective-permute-start | bytes 2162696 | tf_op jit(solution)/shard_map/ppermute | solution.py:458
  270.6 1.6 copy-start
  272.2 1.9 copy-start.15
  272.2 2.7 copy-start.2
  274.1 2.7 collective-permute-start.37
  274.9 1.9 copy-start.12
  274.9 1.9 copy-start.13
where the time goes:
time: 282 us; the launch traced here: 279 us
  Pallas kernels  140 us (50%)
  waiting for transfers between devices  64.1 us (23%)
  starting transfers between devices  48.3 us (17%)
  local copies, waits for them, and re-layouts  14.3 us (5%)
  other arithmetic  11.1 us (4%)
    pallas_call x2, Pallas kernels, chain(): pl.pallas_call(functools.partial(chain_kernel, plan, size, tile), out_sha...  131 us
    ppermute x6, waiting for transfers between devices, scatter(): lax.ppermute(chunk(lax.rem(place + step, size)), 'fs', shift(size, step))  15.8 us
    ppermute x6, starting transfers between devices, spread(): lax.ppermute(piece, 'fs', shift(size, step))  11.7 us
    ppermute x6, starting transfers between devices, scatter(): lax.ppermute(chunk(lax.rem(place + step, size)), 'fs', shift(size, step))  11.3 us
    ppermute x6, waiting for transfers between devices, spread(): lax.ppermute(piece, 'fs', shift(size, step))  11.1 us
    ppermute x1, waiting for transfers between devices, relay(): along_x = lax.ppermute(value, 'tp', swap(4, 1))  7.29 us
    ppermute x6, starting transfers between devices, around(): return [value] + [lax.ppermute(value, 'tp', swap(4, b)) for b in (1, 2, 3)]  6.98 us
    ppermute x1, waiting for transfers between devices, relay(): upper = lax.ppermute(upper, 'tp', swap(4, 1))  6.13 us
  transfers between devices with their start and end apart: 38, of which 17 were waited for; matrix products, arithmetic and copies ran while one was open for 7% of the time, Pallas kernels for 50%

commit v1 on v0

--- a/solution.py
+++ b/solution.py
@@ -48,10 +48,9 @@
 
 
 def chain_kernel(plan, size, tile, place_ref, *refs):
-    count = len(refs) - 5
-    arrays = refs[:count]
-    out_ref, panel, buf, col, sem = refs[count:]
-    n = buf.shape[1]
+    arrays = refs[:-12]
+    out_ref, panel, raw, one, two, three, col_a, col_b, col_c, acc_a, acc_b, sem = refs[-12:]
+    n = raw.shape[0]
     nb = n // 4
     half = nb // 2
     edge = n // tile
@@ -62,7 +61,7 @@
     copies = []
     for index, (b, array, source, height, base, period, step) in enumerate(plan or ()):
         slot = lax.rem(row + (size - step), size)
-        start = pl.multiple_of(base + slot * period, 16)
+        start = pl.multiple_of(base + slot * period, math.gcd(base, period, 16))
         copies.append(
             pltpu.make_async_copy(
                 arrays[array].at[pl.ds(source, height), :],
@@ -77,103 +76,139 @@
 
     bit_x = lax.rem(me, 2)
     bit_y = lax.div(me, 2)
-    eye = lax.broadcasted_iota(jnp.int32, (tile, nb), 0) == lax.broadcasted_iota(
-        jnp.int32, (tile, nb), 1
-    )
-    trace = jnp.zeros((1, 1), F32)
+    quarter = nb // 4
+    base = half + quarter
+    upper = jnp.zeros((half, nb), F32)
+    lower = jnp.zeros((quarter, nb), F32)
     for b in range(4):
-        block = panel[b, 0:nb, :]
-        buf[0, b * nb : (b + 1) * nb, b * nb : (b + 1) * nb] = block
-        picked = jnp.where(eye[0:nb], block.astype(F32), 0.0)
-        trace = trace + jnp.sum(picked, keepdims=True)
+        low, mid = b * nb, b * nb + half
+        part = panel[b, 0:half, :]
+        upper = upper + part.astype(F32)
+        raw[low:mid, low : low + nb] = part
+        raw[mid : mid + half, low:mid] = part[:, half:].T
+        part = panel[b, half:base, :]
+        lower = lower + part.astype(F32)
+        raw[mid : mid + quarter, mid : mid + half] = part[:, 0:half]
+        raw[mid + quarter : mid + half, mid : mid + half] = part[:, half:]
         own_x = bit_x ^ (b & 1)
         own_y = bit_y ^ (b >> 1)
         pairs = ((own_x, b ^ 1, b), (own_y, b ^ 2, b), (own_y, b ^ 2, b ^ 1))
         for index, (flag, high, low) in enumerate(pairs):
-            part = panel[b, nb + index * half : nb + (index + 1) * half, :]
+            part = panel[b, base + index * half : base + (index + 1) * half, :]
             tall = jnp.where(flag == 0, high, low)
             wide = jnp.where(flag == 0, low, high)
             rows = pl.multiple_of(tall * nb + flag * half, half)
             cols = pl.multiple_of(wide * nb, nb)
-            buf[0, pl.ds(rows, half), pl.ds(cols, nb)] = part
-            buf[0, pl.ds(cols, nb), pl.ds(rows, half)] = part.T
-
-    def add_square(i, total):
-        part = buf[0, pl.ds(pl.multiple_of(i * tile, tile), tile), :].astype(F32)
-        return total + jnp.sum(part * part, keepdims=True)
-
-    second = lax.fori_loop(0, edge, add_square, jnp.zeros((1, 1), F32))
+            raw[pl.ds(rows, half), pl.ds(cols, nb)] = part
+            raw[pl.ds(cols, nb), pl.ds(rows, half)] = part.T
+
+    def from_diagonal(value):
+        r = lax.broadcasted_iota(jnp.int32, value.shape, 0)
+        c = lax.broadcasted_iota(jnp.int32, value.shape, 1)
+        kept = (c == r) | ((c == r + half + quarter) & (value.shape[0] == quarter))
+        return jnp.sum(jnp.where(kept, value, 0.0), keepdims=True)
+
+    trace = from_diagonal(upper) + from_diagonal(lower)
+
+    band = 64
+    bands = 9 * quarter // band
+    lane = lax.broadcasted_iota(jnp.int32, (1, nb), 1)
+    mixed = jnp.where(lane < half, 1.0, 2.0)
+
+    def add_square(index, total):
+        start = pl.multiple_of(lax.rem(index, bands) * band, band)
+        part = panel[lax.div(index, bands), pl.ds(start, band), :].astype(F32)
+        weight = jnp.where(start < half, mixed, jnp.where(start < base, 1.0, 2.0))
+        return total + weight * jnp.sum((part * part).reshape(band // 8, 8, nb), axis=0)
+
+    squares = lax.fori_loop(0, 4 * bands, add_square, jnp.zeros((8, nb), F32))
+    second = jnp.sum(squares, keepdims=True)
     ratio = SAFETY * (second + 1.0) / (trace + 1.0)
     inverse = 1.0 / ratio
     scale = lax.rsqrt(ratio)
-    one = jnp.ones((1, 1), F32)
 
     cells = [(i, j) for j in range(edge) for i in range(j, edge)]
 
-    def product(step, carry):
-        which = lax.div(step, len(cells))
-        cell = lax.rem(step, len(cells))
+    def place(cell):
         i = jnp.int32(0)
         j = jnp.int32(0)
         for index, (a, b) in enumerate(cells):
             i = jnp.where(cell == index, a, i)
             j = jnp.where(cell == index, b, j)
-        square = (which == 0) | (which == 3)
-        left = jnp.where(which == 2, 2, 0)
-        right = jnp.where(square, 0, jnp.where(which == 4, 2, 1))
-        into = jnp.where(
-            which == 0, 1, jnp.where(which == 2, 0, jnp.where(which == 4, 3, 2))
-        )
-        linear = jnp.where(square, COEF_THREE, COEF_ONE) * jnp.where(which < 2, inverse, one)
-        quad = jnp.where(square, COEF_FIVE, 1.0) * jnp.where(
-            which == 0, inverse * inverse, jnp.where(which == 1, inverse, one)
-        )
         rows = pl.ds(pl.multiple_of(i * tile, tile), tile)
-        cols = pl.ds(pl.multiple_of(j * tile, tile), tile)
-        acc = dot(buf[left, rows, :], buf[right, :, cols])
-        value = (linear * buf[left, rows, cols].astype(F32) + quad * acc).astype(BF16)
-        buf[into, rows, cols] = value
-
-        @pl.when(i != j)
-        def _():
-            buf[into, cols, rows] = value.T
-
-        return carry
-
-    lax.fori_loop(0, 5 * len(cells), product, 0)
-
-    unit = jnp.where(eye, 1.0, 0.0)
-    col[0] = buf[2, :, 0:nb]
-    col[0, 0:nb, :] = (buf[2, 0:nb, 0:nb].astype(F32) + COEF_ONE * unit[0:nb]).astype(BF16)
-    col[2] = jnp.zeros((n, nb), BF16)
-
-    def column(step, carry):
-        which = lax.div(step, edge)
-        i = lax.rem(step, edge)
-        matrix = jnp.where((which == 0) | (which == 2), 3, 2)
-        source = jnp.where(which == 1, 2, jnp.where(which == 2, 1, 0))
-        into = jnp.where(which == 0, 2, jnp.where(which == 2, 0, 1))
-        alpha = jnp.where((which == 0) | (which == 2), 0.0, COEF_ONE)
-        beta = jnp.where(which == 2, COEF_FIVE, 1.0)
-        gamma = jnp.where(which == 2, COEF_THREE, 0.0)
-        delta = jnp.where((which == 2) & (i == 0), COEF_ONE, 0.0)
-        rows = pl.ds(pl.multiple_of(i * tile, tile), tile)
-        acc = dot(buf[matrix, rows, :], col[source])
-        value = alpha * col[source, rows, :].astype(F32) + beta * acc
-        value = value + gamma * col[2, rows, :].astype(F32) + delta * unit
-        col[into, rows, :] = value.astype(BF16)
-        return carry
-
-    lax.fori_loop(0, 4 * edge, column, 0)
-
-    def last(i, carry):
-        rows = pl.ds(pl.multiple_of(i * tile, tile), tile)
-        acc = dot(buf[1, rows, :], col[1])
-        value = scale * (COEF_ONE * col[1, rows, :].astype(F32) + acc)
-        out_ref[rows, :] = value.astype(BF16)
-        return carry
-
-    lax.fori_loop(0, edge, last, 0)
+        return rows, pl.ds(pl.multiple_of(j * tile, tile), tile)
+
+    def product(left, right, into, linear, quad):
+        def multiply(cell, acc):
+            rows, cols = place(cell)
+            acc[...] = dot(left[rows, :], right[:, cols])
+
+        def finish(cell, acc):
+            rows, cols = place(cell)
+            value = linear * left[rows, cols].astype(F32) + quad * acc[...]
+            value = value.astype(BF16)
+            into[rows, cols] = value
+            into[cols, rows] = value.T
+
+        def pair(k, carry):
+            multiply(2 * k, acc_a)
+            finish(2 * k - 1, acc_b)
+            multiply(2 * k + 1, acc_b)
+            finish(2 * k, acc_a)
+            return carry
+
+        def single(cell, carry):
+            multiply(cell, acc_a)
+            finish(cell, acc_a)
+            return carry
+
+        count = len(cells)
+        if count % 2:
+            lax.fori_loop(0, count, single, 0)
+        else:
+            lax.fori_loop(0, count // 2, pair, 0)
+            finish(count - 1, acc_b)
+
+    acc_b[...] = jnp.zeros_like(acc_b)
+    product(raw, raw, one, COEF_THREE * inverse, COEF_FIVE * inverse * inverse)
+    product(raw, one, two, COEF_ONE * inverse, inverse)
+    product(two, one, raw, COEF_ONE, 1.0)
+    product(raw, raw, two, COEF_THREE, COEF_FIVE)
+    product(raw, two, three, COEF_ONE, 1.0)
+
+    unit = jnp.where(
+        lax.broadcasted_iota(jnp.int32, (nb, nb), 0)
+        == lax.broadcasted_iota(jnp.int32, (nb, nb), 1),
+        COEF_ONE,
+        0.0,
+    )
+
+    def column(matrix, source, into, finish):
+        def body(i, carry):
+            rows = pl.ds(pl.multiple_of(i * tile, tile), tile)
+            into[rows, :] = finish(dot(matrix[rows, :], source[...]), rows).astype(BF16)
+            return carry
+
+        lax.fori_loop(0, edge, body, 0)
+
+    col_a[...] = two[:, 0:nb]
+    col_a[0:nb, :] = (col_a[0:nb, :].astype(F32) + unit).astype(BF16)
+    column(three, col_a, col_c, lambda acc, rows: acc)
+    column(two, col_c, col_b, lambda acc, rows: COEF_ONE * col_c[rows, :].astype(F32) + acc)
+    column(
+        three,
+        col_b,
+        col_a,
+        lambda acc, rows: COEF_THREE * col_c[rows, :].astype(F32) + COEF_FIVE * acc,
+    )
+    col_a[0:nb, :] = (col_a[0:nb, :].astype(F32) + unit).astype(BF16)
+    column(two, col_a, col_b, lambda acc, rows: COEF_ONE * col_a[rows, :].astype(F32) + acc)
+    column(
+        one,
+        col_b,
+        out_ref,
+        lambda acc, rows: scale * (COEF_ONE * col_b[rows, :].astype(F32) + acc),
+    )
 
 
 def chain(plan, arrays, place, size, n):
@@ -187,9 +222,10 @@
         + [pl.BlockSpec(memory_space=pl.ANY if plan else pltpu.VMEM)] * len(arrays),
         out_specs=pl.BlockSpec(memory_space=pltpu.VMEM),
         scratch_shapes=[
-            pltpu.VMEM((4, 5 * nb // 2, nb), BF16),
-            pltpu.VMEM((4, n, n), BF16),
-            pltpu.VMEM((3, n, nb), BF16),
+            pltpu.VMEM((4, 9 * nb // 4, nb), BF16),
+            *[pltpu.VMEM((n, n), BF16)] * 4,
+            *[pltpu.VMEM((n, nb), BF16)] * 3,
+            *[pltpu.VMEM((tile, tile), F32)] * 2,
             pltpu.SemaphoreType.DMA((len(plan or (0,)),)),
         ],
         compiler_params=pltpu.CompilerParams(
@@ -231,7 +267,12 @@
         value = ref[...]
         part = dot(value.T, value)
         total = part if total is None else total + part
-    out_ref[...] = total.astype(BF16)
+    total = total.astype(BF16)
+    half = total.shape[0] // 2
+    base = half + half // 2
+    out_ref[0:half, :] = total[0:half]
+    out_ref[half:base, 0:half] = total[half:base, half:]
+    out_ref[half:base, half:] = total[base:, half:]
 
 
 def own_gram(blocks):
@@ -239,7 +280,7 @@
     flops = sum(2 * block.shape[0] * nb * nb for block in blocks)
     return pl.pallas_call(
         own_kernel,
-        out_shape=jax.ShapeDtypeStruct((nb, nb), BF16),
+        out_shape=jax.ShapeDtypeStruct((3 * nb // 4, nb), BF16),
         compiler_params=pltpu.CompilerParams(vmem_limit_bytes=16 * 2**20),
         cost_estimate=pl.CostEstimate(flops=flops, bytes_accessed=2**20, transcendentals=0),
     )(*blocks)
@@ -399,8 +440,9 @@
     mine = mine.astype(BF16)
     mine = jnp.concatenate([mine[:fold], mine[fold:]], axis=1)
     diagonal = own_gram([keep, gift])
-    nb = diagonal.shape[0]
-    part = nb // f_size
+    nb = diagonal.shape[1]
+    base = diagonal.shape[0]
+    part = base // f_size
     tail = fold // f_size
 
     def chunk(index):
@@ -429,7 +471,9 @@
     own_groups = around(piece)
     rest_parts = pack(rest_parts, piece, height)
     rest_groups = around(rest_parts)
-    spreads = jnp.stack([group[nb:] for group in first_groups[:3]] + [first_groups[4][nb - split :]])
+    spreads = jnp.stack(
+        [group[base:] for group in first_groups[:3]] + [first_groups[4][base - split :]]
+    )
     others = lax.ppermute(spreads, "rep", cross)
     n = 4 * small.shape[1]
     small_q = chain(None, [spreads, others], place, f_size, n)
@@ -450,9 +494,9 @@
             else:
                 plan.append((b, 3, low, split - low, 0, part, step))
                 plan.append((b, 4, 0, high - split, split - low, part, step))
-        plan.append((b, 5 + b, 0, height, nb, height, 0))
+        plan.append((b, 5 + b, 0, height, base, height, 0))
         for step in range(1, f_size):
-            plan.append((b, 9 + b, (step - 1) * height, height, nb, height, step))
+            plan.append((b, 9 + b, (step - 1) * height, height, base, height, step))
     both_q = chain(plan, [*first_groups, *own_groups, *rest_groups], place, f_size, n)
 
     gift_d = lax.ppermute(gift, "tp", swap(4, 3))

time: 282 us -> 257 us (0.911)
  Pallas kernels: 140 us -> 127 us
  waiting for transfers between devices: 64.1 us -> 60.1 us
  local copies, waits for them, and re-layouts: 14.3 us -> 10.7 us
    pallas_call x2, Pallas kernels: 131 us -> 117 us  [chain(): pl.pallas_call(functools.partial(chain_kernel, plan, size, tile), out_sha...]
    ppermute x1, waiting for transfers between devices: 5.54 us -> 0.01 us  [update(): gift_x = lax.ppermute(gift, 'tp', swap(4, 1))]
    ppermute x1, waiting for transfers between devices: 0.25 us -> 4.56 us  [update(): gift_y = lax.ppermute(gift, 'tp', swap(4, 2))]
    ppermute x6, waiting for transfers between devices: 3.92 us -> 0.02 us  [around(): return [value] + [lax.ppermute(value, 'tp', swap(4, b)) for b in (1, 2, 3)]]
    ppermute x6, waiting for transfers between devices: 11.1 us -> 15 us  [spread(): lax.ppermute(piece, 'fs', shift(size, step))]
    ppermute x1, waiting for transfers between devices: 7.29 us -> 3.98 us  [relay(): along_x = lax.ppermute(value, 'tp', swap(4, 1))]
  transfers between devices with their start and end apart: 38 -> 38, of which waited for: 17 -> 15; matrix products, arithmetic and copies ran while one was open for 7% -> 5% of each run, Pallas kernels for 50% -> 49%
where the time goes in v1:
time: 257 us; the launch traced here: 256 us
  Pallas kernels  127 us (49%)
  waiting for transfers between devices  60.1 us (23%)
  starting transfers between devices  48.4 us (19%)
  local copies, waits for them, and re-layouts  10.7 us (4%)
  other arithmetic  8.94 us (3%)
    pallas_call x2, Pallas kernels, chain(): pl.pallas_call(functools.partial(chain_kernel, plan, size, tile), out_sha...  117 us
    ppermute x6, waiting for transfers between devices, scatter(): lax.ppermute(chunk(lax.rem(place + step, size)), 'fs', shift(size, step))  15.7 us
    ppermute x6, waiting for transfers between devices, spread(): lax.ppermute(piece, 'fs', shift(size, step))  15 us
    ppermute x6, starting transfers between devices, spread(): lax.ppermute(piece, 'fs', shift(size, step))  10.6 us
    ppermute x6, starting transfers between devices, scatter(): lax.ppermute(chunk(lax.rem(place + step, size)), 'fs', shift(size, step))  10.3 us
    ppermute x1, waiting for transfers between devices, relay(): upper = lax.ppermute(upper, 'tp', swap(4, 1))  7.87 us
    ppermute x6, starting transfers between devices, around(): return [value] + [lax.ppermute(value, 'tp', swap(4, b)) for b in (1, 2, 3)]  7.56 us
    convert_element_type x3, local copies, waits for them, and re-layouts, half_sum(): return (mine, theirs.astype(BF16))  5.74 us
  transfers between devices with their start and end apart: 38, of which 15 were waited for; matrix products, arithmetic and copies ran while one was open for 5% of the time, Pallas kernels for 49%

profile of v1, /device:TPU:0, one launch (start us, length us, event | category | flops | bytes accessed | tf_op | source)
XLA Modules:
  0.0 256.3 jit_solution(5992256780260538292)
XLA Ops:
  0.6 2.4 fusion.3
  3.5 2.3 fusion.2
  5.8 1.1 fusion.7
  7.4 1.0 collective-permute-done.19
  8.4 1.7 fusion.12
  10.1 2.8 %collective-permute-start.21 = (bf16[256,256]{1,0:T(8,128)(2,1)S(1)}, bf16[256,256]{1,0:T(8,128)(2,1)S(1)}, u32[]{:S(2)}, u32[]{:S(2)}) collective-permute-start(bf16[256,256]{1,0:T(8,128)(2,1)S(1)} %get-tuple-element.38.refs_0_.a_ref), channel_id=1, source_target_pairs={{0,4},{2,6},{4,0},{6,2},{1,5},{3,7},{5,1},{7,3},{8,12},{10,14},{12... | collective-permute-start | bytes 393224 | tf_op jit(solution)/shard_map/ppermute | solution.py:424
  12.9 1.5 collective-permute-start.20
  14.7 2.1 collective-permute-done.21.refs_2_.c_ref
  16.8 1.5 collective-permute-done.20.refs_1_.b_ref
  18.2 1.0 shard_map.140
  19.6 3.1 %broadcast_select_fusion = (bf16[704,512]{1,0:T(8,128)(2,1)S(1)}, f32[704,512]{1,0:T(8,128)S(1)}, f32[704,512]{1,0:T(8,128)S(1)}) fusion(pred[]{:T(512)S(6)} %eq.2, bf16[704,512]{1,0:T(8,128)(2,1)S(1)} %collective-permute-done.1, f32[1,1408,512]{2,1,0:T(8,128)} %param.12, s32[]{:T(128)S(6)} %select_n.76, f32[704,512]{1,0:T(8,128)S(1)} %copy-done.14, ...), kind=kLoop, calls=%fused_computation.10 | loop fusion | flops 3964928 | bytes 10813445 | tf_op jit(solution)/shard_map/jit(_where)/select_n | solution.py:422
  22.7 0.5 collective-permute-start.2
  24.5 1.7 collective-permute-start.3
  26.3 1.0 shard_map.138
  27.3 1.6 collective-permute-start.6
  28.9 0.5 collective-permute-start.4
  29.4 1.6 collective-permute-start.23
  31.1 5.3 %collective-permute-done.23 = bf16[132,512]{1,0:T(8,128)(2,1)S(1)} collective-permute-done((bf16[132,512]{1,0:T(8,128)(2,1)S(1)}, bf16[132,512]{1,0:T(8,128)(2,1)S(1)}, u32[]{:S(2)}, u32[]{:S(2)}) %collective-permute-start.23) | collective-permute-done | bytes 135200 | tf_op jit(solution)/shard_map/ppermute | solution.py:339
  36.4 0.8 collective-permute-start.24
  37.2 6.4 %collective-permute-done.24 = bf16[132,512]{1,0:T(8,128)(2,1)S(1)} collective-permute-done((bf16[132,512]{1,0:T(8,128)(2,1)S(1)}, bf16[132,512]{1,0:T(8,128)(2,1)S(1)}, u32[]{:S(2)}, u32[]{:S(2)}) %collective-permute-start.24) | collective-permute-done | bytes 135200 | tf_op jit(solution)/shard_map/ppermute | solution.py:339
  43.5 2.5 collective-permute-start.25
  46.0 2.6 %collective-permute-done.25 = bf16[132,512]{1,0:T(8,128)(2,1)S(1)} collective-permute-done((bf16[132,512]{1,0:T(8,128)(2,1)S(1)}, bf16[132,512]{1,0:T(8,128)(2,1)S(1)}, u32[]{:S(2)}, u32[]{:S(2)}) %collective-permute-start.25) | collective-permute-done | bytes 135200 | tf_op jit(solution)/shard_map/ppermute | solution.py:339
  48.7 4.3 %collective-permute-start.28 = (bf16[132,512]{1,0:T(8,128)(2,1)S(1)}, bf16[132,512]{1,0:T(8,128)(2,1)S(1)}, u32[]{:S(2)}, u32[]{:S(2)}) collective-permute-start(bf16[132,512]{1,0:T(8,128)(2,1)S(1)} %add_convert_fusion.2.refs_0_), channel_id=1, source_target_pairs={{0,24},{8,0},{16,8},{24,16},{1,25},{9,1},{17,9},{25,17},{2,26},{10... | collective-permute-start | bytes 405512 | tf_op jit(solution)/shard_map/ppermute | solution.py:352
  53.0 0.6 collective-permute-start.26
  53.7 4.6 %collective-permute-done.6.refs_5_.c_ref = bf16[704,512]{1,0:T(8,128)(2,1)S(1)} collective-permute-done((bf16[704,512]{1,0:T(8,128)(2,1)S(1)}, bf16[704,512]{1,0:T(8,128)(2,1)S(1)}, u32[]{:S(2)}, u32[]{:S(2)}) %collective-permute-start.6) | collective-permute-done | bytes 720928 | tf_op jit(solution)/shard_map/ppermute | solution.py:430
  58.2 2.2 shard_map.136.refs_4_
  60.4 1.8 collective-permute-done.27.refs_2_
  62.2 0.8 shard_map.141.refs_0_
  63.0 1.5 collective-permute-start.29
  65.1 1.5 collective-permute-start.7
  66.6 2.4 collective-permute-start.9
  69.0 1.6 collective-permute-start.8
  70.5 0.9 slice_bitcast_fusion.3
  71.4 4.0 %collective-permute-done.29.refs_1_ = bf16[528,512]{1,0:T(8,128)(2,1)} collective-permute-done((bf16[528,512]{1,0:T(8,128)(2,1)}, bf16[528,512]{1,0:T(8,128)(2,1)}, u32[]{:S(2)}, u32[]{:S(2)}) %collective-permute-start.29) | collective-permute-done | bytes 540704 | tf_op jit(solution)/shard_map/ppermute | solution.py:384
  75.4 1.0 slice.35
  76.4 1.9 collective-permute-start.32
  78.3 0.9 slice_bitcast_fusion.2
  79.2 3.7 %collective-permute-done.32.refs_4_ = bf16[272,512]{1,0:T(8,128)(2,1)S(1)} collective-permute-done((bf16[272,512]{1,0:T(8,128)(2,1)S(1)}, bf16[272,512]{1,0:T(8,128)(2,1)S(1)}, u32[]{:S(2)}, u32[]{:S(2)}) %collective-permute-start.32) | collective-permute-done | bytes 278560 | tf_op jit(solution)/shard_map/ppermute | solution.py:388
  83.2 1.5 collective-permute-done.8
  84.8 2.8 %collective-permute-start.15 = (bf16[192,512]{1,0:T(8,128)(2,1)S(1)}, bf16[192,512]{1,0:T(8,128)(2,1)S(1)}, u32[]{:S(2)}, u32[]{:S(2)}) collective-permute-start(bf16[192,512]{1,0:T(8,128)(2,1)S(1)} %add_convert_fusion.refs_3_.refs_5_), channel_id=1, source_target_pairs={{0,24},{8,0},{16,8},{24,16},{1,25},{9,1},{17,9},{25,17},{2,26},{10... | collective-permute-start | bytes 589832 | tf_op jit(solution)/shard_map/ppermute | solution.py:352
  87.6 0.9 collective-permute-start.14
  88.5 1.9 collective-permute-start.13
  90.5 1.4 collective-permute-start.12
  91.9 1.1 collective-permute-done.15.refs_2_
  93.0 1.5 collective-permute-start.11
  94.6 12.1 %collective-permute-done.14.refs_1_ = bf16[192,512]{1,0:T(8,128)(2,1)S(1)} collective-permute-done((bf16[192,512]{1,0:T(8,128)(2,1)S(1)}, bf16[192,512]{1,0:T(8,128)(2,1)S(1)}, u32[]{:S(2)}, u32[]{:S(2)}) %collective-permute-start.14) | collective-permute-done | bytes 196640 | tf_op jit(solution)/shard_map/ppermute | solution.py:352
  106.6 1.4 collective-permute-start.33
  108.1 1.1 collective-permute-start.10
  109.3 4.6 %collective-permute-done.33.d_ref = bf16[256,256]{1,0:T(8,128)(2,1)S(1)} collective-permute-done((bf16[256,256]{1,0:T(8,128)(2,1)S(1)}, bf16[256,256]{1,0:T(8,128)(2,1)S(1)}, u32[]{:S(2)}, u32[]{:S(2)}) %collective-permute-start.33) | collective-permute-done | bytes 131104 | tf_op jit(solution)/shard_map/ppermute | solution.py:425
  113.9 1.4 collective-permute-start.18
  115.3 1.5 collective-permute-start.17
  116.9 0.5 collective-permute-start.16
  117.4 1.5 collective-permute-start.31
  118.9 20.2 %shard_map.142.q_ref = bf16[1024,256]{1,0:T(8,128)(2,1)S(1)} custom-call(s32[3]{0:T(128)S(1)} %pad_add_fusion.place_ref, bf16[4,144,512]{2,1,0:T(8,128)(2,1)S(1)} %pad_maximum_fusion.refs_0_, bf16[4,144,512]{2,1,0:T(8,128)(2,1)S(1)} %collective-permute-done.34.refs_1_), custom_call_target="tpu_custom_call" | custom-call | flops 10737418240 | bytes 1572864 | tf_op jit(solution)/shard_map/pallas_call | solution.py:218
  139.2 0.5 shard_map.143
  139.7 7.9 %collective-permute-done.31.refs_3_ = bf16[256,512]{1,0:T(8,128)(2,1)S(1)} collective-permute-done((bf16[256,512]{1,0:T(8,128)(2,1)S(1)}, bf16[256,512]{1,0:T(8,128)(2,1)S(1)}, u32[]{:S(2)}, u32[]{:S(2)}) %collective-permute-start.31) | collective-permute-done | bytes 262176 | tf_op jit(solution)/shard_map/ppermute | solution.py:387
  147.6 2.0 collective-permute-start.35
  149.6 1.0 collective-permute-start.36
  150.6 97.3 %shard_map.144.q_ref = bf16[2048,512]{1,0:T(8,128)(2,1)} custom-call(s32[3]{0:T(128)} %copy-done.9, bf16[528,512]{1,0:T(8,128)(2,1)} %shard_map.141.refs_0_, bf16[528,512]{1,0:T(8,128)(2,1)} %collective-permute-done.29.refs_1_, bf16[528,512]{1,0:T(8,128)(2,1)} %copy-done.15, bf16[256,512]{1,0:T(8,128)(2,1)} %copy-done.22, bf16[272,512]{1,0:T(8,128)(2,1)} %copy-done.18, ...), custom_call_target="tpu_custom_call" | custom-call | flops 85899345920 | bytes 6291456 | tf_op jit(solution)/shard_map/pallas_call | solution.py:218
  248.0 1.6 copy-done
  249.6 1.8 shard_map.146
  251.5 0.7 multiply_subtract_fusion.2
  252.2 1.8 shard_map.145
  254.1 2.1 multiply_subtract_fusion
  (102 shorter events, 4.1 us)
Async XLA Ops:
  0.6 7.8 %copy-start.17 = (f32[256,256]{1,0:T(8,128)S(1)}, f32[256,256]{1,0:T(8,128)}, u32[]{:S(2)}) copy-start(f32[256,256]{1,0:T(8,128)} %param.16) | copy-start | bytes 786436
  3.0 16.5 %collective-permute-start.1 = (bf16[704,512]{1,0:T(8,128)(2,1)}, bf16[704,512]{1,0:T(8,128)(2,1)S(1)}, u32[]{:S(2)}, u32[]{:S(2)}) collective-permute-start(bf16[704,512]{1,0:T(8,128)(2,1)} %fusion.3), channel_id=1, source_target_pairs={{0,1},{1,0},{2,3},{3,2},{4,5},{5,4},{6,7},{7,6},{8,9},{9,8},{10,11... | collective-permute-start | bytes 2162696 | tf_op jit(solution)/shard_map/ppermute | solution.py:414
  5.8 13.7 %copy-start.14 = (f32[704,512]{1,0:T(8,128)S(1)}, f32[704,512]{1,0:T(8,128)}, u32[]{:S(2)}) copy-start(f32[704,512]{1,0:T(8,128)} %param.13) | copy-start | bytes 4325380
  5.8 13.7 %collective-permute-start = (bf16[704,512]{1,0:T(8,128)(2,1)}, bf16[704,512]{1,0:T(8,128)(2,1)S(1)}, u32[]{:S(2)}, u32[]{:S(2)}) collective-permute-start(bf16[704,512]{1,0:T(8,128)(2,1)} %fusion.2), channel_id=1, source_target_pairs={{0,1},{1,0},{2,3},{3,2},{4,5},{5,4},{6,7},{7,6},{8,9},{9,8},{10,11... | collective-permute-start | bytes 2162696 | tf_op jit(solution)/shard_map/ppermute | solution.py:414
  6.9 1.5 collective-permute-start.19
  10.1 6.7 %collective-permute-start.21 = (bf16[256,256]{1,0:T(8,128)(2,1)S(1)}, bf16[256,256]{1,0:T(8,128)(2,1)S(1)}, u32[]{:S(2)}, u32[]{:S(2)}) collective-permute-start(bf16[256,256]{1,0:T(8,128)(2,1)S(1)} %get-tuple-element.38.refs_0_.a_ref), channel_id=1, source_target_pairs={{0,4},{2,6},{4,0},{6,2},{1,5},{3,7},{5,1},{7,3},{8,12},{10,14},{12... | collective-permute-start | bytes 393224 | tf_op jit(solution)/shard_map/ppermute | solution.py:424
  12.9 5.3 %collective-permute-start.20 = (bf16[256,256]{1,0:T(8,128)(2,1)S(1)}, bf16[256,256]{1,0:T(8,128)(2,1)S(1)}, u32[]{:S(2)}, u32[]{:S(2)}) collective-permute-start(bf16[256,256]{1,0:T(8,128)(2,1)S(1)} %get-tuple-element.38.refs_0_.a_ref), channel_id=1, source_target_pairs={{0,2},{2,0},{4,6},{6,4},{1,3},{3,1},{5,7},{7,5},{8,10},{10,8},{12,... | collective-permute-start | bytes 393224 | tf_op jit(solution)/shard_map/ppermute | solution.py:423
  14.5 104.4 %copy-start.9 = (s32[3]{0:T(128)}, s32[3]{0:T(128)S(1)}, u32[]{:S(2)}) copy-start(s32[3]{0:T(128)S(1)} %pad_add_fusion.place_ref) | copy-start | bytes 40
  19.4 3.8 %collective-permute-start.22 = (bf16[288,256]{1,0:T(8,128)(2,1)S(1)}, bf16[288,256]{1,0:T(8,128)(2,1)S(1)}, u32[]{:S(2)}, u32[]{:S(2)}) collective-permute-start(bf16[288,256]{1,0:T(8,128)(2,1)S(1)} %fusion.5), channel_id=1, source_target_pairs={{0,1},{1,0},{2,3},{3,2},{4,5},{5,4},{6,7},{7,6},{8,9},{9,8},{10,11... | collective-permute-start | bytes 442376 | tf_op jit(solution)/shard_map/ppermute | solution.py:439
  22.7 1.3 copy-start.10
  22.7 1.6 copy-start.11
  22.7 3.6 %collective-permute-start.2 = (bf16[704,512]{1,0:T(8,128)(2,1)S(1)}, bf16[704,512]{1,0:T(8,128)(2,1)S(1)}, u32[]{:S(2)}, u32[]{:S(2)}) collective-permute-start(bf16[704,512]{1,0:T(8,128)(2,1)S(1)} %get-tuple-element.40), channel_id=1, source_target_pairs={{0,1},{1,0},{2,3},{3,2},{4,5},{5,4},{6,7},{7,6},{8,9},{9,8},{10,11... | collective-permute-start | bytes 2162696 | tf_op jit(solution)/shard_map/ppermute | solution.py:428
  24.2 28.8 %collective-permute-start.5 = (bf16[704,512]{1,0:T(8,128)(2,1)S(1)}, bf16[704,512]{1,0:T(8,128)(2,1)S(1)}, u32[]{:S(2)}, u32[]{:S(2)}) collective-permute-start(bf16[704,512]{1,0:T(8,128)(2,1)S(1)} %broadcast_select_fusion.1.refs_0_.a_ref), channel_id=1, source_target_pairs={{0,4},{2,6},{4,0},{6,2},{1,5},{3,7},{5,1},{7,3},{8,12},{10,14},{12... | collective-permute-start | bytes 2162696 | tf_op jit(solution)/shard_map/ppermute | solution.py:427
  24.5 28.5 %collective-permute-start.3 = (bf16[704,512]{1,0:T(8,128)(2,1)S(1)}, bf16[704,512]{1,0:T(8,128)(2,1)S(1)}, u32[]{:S(2)}, u32[]{:S(2)}) collective-permute-start(bf16[704,512]{1,0:T(8,128)(2,1)S(1)} %broadcast_select_fusion.1.refs_0_.a_ref), channel_id=1, source_target_pairs={{0,2},{2,0},{4,6},{6,4},{1,3},{3,1},{5,7},{7,5},{8,10},{10,8},{12,... | collective-permute-start | bytes 2162696 | tf_op jit(solution)/shard_map/ppermute | solution.py:426
  27.3 30.9 %collective-permute-start.6 = (bf16[704,512]{1,0:T(8,128)(2,1)S(1)}, bf16[704,512]{1,0:T(8,128)(2,1)S(1)}, u32[]{:S(2)}, u32[]{:S(2)}) collective-permute-start(bf16[704,512]{1,0:T(8,128)(2,1)S(1)} %collective-permute-done.2.refs_1_.a_ref), channel_id=1, source_target_pairs={{0,4},{2,6},{4,0},{6,2},{1,5},{3,7},{5,1},{7,3},{8,12},{10,14},{12... | collective-permute-start | bytes 2162696 | tf_op jit(solution)/shard_map/ppermute | solution.py:430
  28.9 29.3 %collective-permute-start.4 = (bf16[704,512]{1,0:T(8,128)(2,1)S(1)}, bf16[704,512]{1,0:T(8,128)(2,1)S(1)}, u32[]{:S(2)}, u32[]{:S(2)}) collective-permute-start(bf16[704,512]{1,0:T(8,128)(2,1)S(1)} %collective-permute-done.2.refs_1_.a_ref), channel_id=1, source_target_pairs={{0,2},{2,0},{4,6},{6,4},{1,3},{3,1},{5,7},{7,5},{8,10},{10,8},{12,... | collective-permute-start | bytes 2162696 | tf_op jit(solution)/shard_map/ppermute | solution.py:429
  29.4 6.9 %collective-permute-start.23 = (bf16[132,512]{1,0:T(8,128)(2,1)S(1)}, bf16[132,512]{1,0:T(8,128)(2,1)S(1)}, u32[]{:S(2)}, u32[]{:S(2)}) collective-permute-start(bf16[132,512]{1,0:T(8,128)(2,1)S(1)} %pad_maximum_fusion.1), channel_id=1, source_target_pairs={{0,8},{8,16},{16,24},{24,0},{1,9},{9,17},{17,25},{25,1},{2,10},{10... | collective-permute-start | bytes 405512 | tf_op jit(solution)/shard_map/ppermute | solution.py:339
  36.4 7.2 %collective-permute-start.24 = (bf16[132,512]{1,0:T(8,128)(2,1)S(1)}, bf16[132,512]{1,0:T(8,128)(2,1)S(1)}, u32[]{:S(2)}, u32[]{:S(2)}) collective-permute-start(bf16[132,512]{1,0:T(8,128)(2,1)S(1)} %pad_maximum_fusion.2), channel_id=1, source_target_pairs={{0,16},{8,24},{16,0},{24,8},{1,17},{9,25},{17,1},{25,9},{2,18},{10... | collective-permute-start | bytes 405512 | tf_op jit(solution)/shard_map/ppermute | solution.py:339
  43.5 5.1 %collective-permute-start.25 = (bf16[132,512]{1,0:T(8,128)(2,1)S(1)}, bf16[132,512]{1,0:T(8,128)(2,1)S(1)}, u32[]{:S(2)}, u32[]{:S(2)}) collective-permute-start(bf16[132,512]{1,0:T(8,128)(2,1)S(1)} %pad_maximum_fusion.3), channel_id=1, source_target_pairs={{0,24},{8,0},{16,8},{24,16},{1,25},{9,1},{17,9},{25,17},{2,26},{10... | collective-permute-start | bytes 405512 | tf_op jit(solution)/shard_map/ppermute | solution.py:339
  48.7 11.7 %collective-permute-start.28 = (bf16[132,512]{1,0:T(8,128)(2,1)S(1)}, bf16[132,512]{1,0:T(8,128)(2,1)S(1)}, u32[]{:S(2)}, u32[]{:S(2)}) collective-permute-start(bf16[132,512]{1,0:T(8,128)(2,1)S(1)} %add_convert_fusion.2.refs_0_), channel_id=1, source_target_pairs={{0,24},{8,0},{16,8},{24,16},{1,25},{9,1},{17,9},{25,17},{2,26},{10... | collective-permute-start | bytes 405512 | tf_op jit(solution)/shard_map/ppermute | solution.py:352
  53.0 9.2 %collective-permute-start.27 = (bf16[132,512]{1,0:T(8,128)(2,1)S(1)}, bf16[132,512]{1,0:T(8,128)(2,1)S(1)}, u32[]{:S(2)}, u32[]{:S(2)}) collective-permute-start(bf16[132,512]{1,0:T(8,128)(2,1)S(1)} %add_convert_fusion.2.refs_0_), channel_id=1, source_target_pairs={{0,16},{8,24},{16,0},{24,8},{1,17},{9,25},{17,1},{25,9},{2,18},{10... | collective-permute-start | bytes 405512 | tf_op jit(solution)/shard_map/ppermute | solution.py:352
  53.0 7.4 %copy-start.1 = (bf16[704,512]{1,0:T(8,128)(2,1)}, bf16[704,512]{1,0:T(8,128)(2,1)S(1)}, u32[]{:S(2)}) copy-start(bf16[704,512]{1,0:T(8,128)(2,1)S(1)} %collective-permute-done.3.refs_2_.b_ref) | copy-start | bytes 2162692
  53.0 9.2 %collective-permute-start.26 = (bf16[132,512]{1,0:T(8,128)(2,1)S(1)}, bf16[132,512]{1,0:T(8,128)(2,1)S(1)}, u32[]{:S(2)}, u32[]{:S(2)}) collective-permute-start(bf16[132,512]{1,0:T(8,128)(2,1)S(1)} %add_convert_fusion.2.refs_0_), channel_id=1, source_target_pairs={{0,8},{8,16},{16,24},{24,0},{1,9},{9,17},{17,25},{25,1},{2,10},{10... | collective-permute-start | bytes 405512 | tf_op jit(solution)/shard_map/ppermute | solution.py:352
  58.2 2.2 copy-start.3
  58.2 2.2 copy-start.5
  63.0 12.4 %collective-permute-start.29 = (bf16[528,512]{1,0:T(8,128)(2,1)}, bf16[528,512]{1,0:T(8,128)(2,1)}, u32[]{:S(2)}, u32[]{:S(2)}) collective-permute-start(bf16[528,512]{1,0:T(8,128)(2,1)} %shard_map.141.refs_0_), channel_id=1, source_target_pairs={{0,2},{2,0},{4,6},{6,4},{1,3},{3,1},{5,7},{7,5},{8,10},{10,8},{12,... | collective-permute-start | bytes 1622024 | tf_op jit(solution)/shard_map/ppermute | solution.py:384
  64.5 14.7 %collective-permute-start.30 = (bf16[528,512]{1,0:T(8,128)(2,1)}, bf16[528,512]{1,0:T(8,128)(2,1)S(1)}, u32[]{:S(2)}, u32[]{:S(2)}) collective-permute-start(bf16[528,512]{1,0:T(8,128)(2,1)} %shard_map.141.refs_0_), channel_id=1, source_target_pairs={{0,4},{2,6},{4,0},{6,2},{1,5},{3,7},{5,1},{7,3},{8,12},{10,14},{12... | collective-permute-start | bytes 1622024 | tf_op jit(solution)/shard_map/ppermute | solution.py:385
  65.1 18.1 %collective-permute-start.7 = (bf16[192,512]{1,0:T(8,128)(2,1)S(1)}, bf16[192,512]{1,0:T(8,128)(2,1)S(1)}, u32[]{:S(2)}, u32[]{:S(2)}) collective-permute-start(bf16[192,512]{1,0:T(8,128)(2,1)S(1)} %get-tuple-element.45), channel_id=1, source_target_pairs={{0,8},{8,16},{16,24},{24,0},{1,9},{9,17},{17,25},{25,1},{2,10},{10... | collective-permute-start | bytes 589832 | tf_op jit(solution)/shard_map/ppermute | solution.py:339
  66.6 16.6 %collective-permute-start.9 = (bf16[192,512]{1,0:T(8,128)(2,1)S(1)}, bf16[192,512]{1,0:T(8,128)(2,1)S(1)}, u32[]{:S(2)}, u32[]{:S(2)}) collective-permute-start(bf16[192,512]{1,0:T(8,128)(2,1)S(1)} %get-tuple-element.46), channel_id=1, source_target_pairs={{0,24},{8,0},{16,8},{24,16},{1,25},{9,1},{17,9},{25,17},{2,26},{10... | collective-permute-start | bytes 589832 | tf_op jit(solution)/shard_map/ppermute | solution.py:339
  69.0 15.8 %collective-permute-start.8 = (bf16[192,512]{1,0:T(8,128)(2,1)S(1)}, bf16[192,512]{1,0:T(8,128)(2,1)S(1)}, u32[]{:S(2)}, u32[]{:S(2)}) collective-permute-start(bf16[192,512]{1,0:T(8,128)(2,1)S(1)} %get-tuple-element.47), channel_id=1, source_target_pairs={{0,16},{8,24},{16,0},{24,8},{1,17},{9,25},{17,1},{25,9},{2,18},{10... | collective-permute-start | bytes 589832 | tf_op jit(solution)/shard_map/ppermute | solution.py:339
  76.4 6.6 %collective-permute-start.32 = (bf16[272,512]{1,0:T(8,128)(2,1)S(1)}, bf16[272,512]{1,0:T(8,128)(2,1)S(1)}, u32[]{:S(2)}, u32[]{:S(2)}) collective-permute-start(bf16[272,512]{1,0:T(8,128)(2,1)S(1)} %slice.35), channel_id=1, source_target_pairs={{0,4},{2,6},{4,0},{6,2},{1,5},{3,7},{5,1},{7,3},{8,12},{10,14},{12... | collective-permute-start | bytes 835592 | tf_op jit(solution)/shard_map/ppermute | solution.py:388
  79.2 30.0 %copy-start.15 = (bf16[528,512]{1,0:T(8,128)(2,1)}, bf16[528,512]{1,0:T(8,128)(2,1)S(1)}, u32[]{:S(2)}) copy-start(bf16[528,512]{1,0:T(8,128)(2,1)S(1)} %collective-permute-done.30.refs_2_) | copy-start | bytes 1622020
  83.0 26.2 %copy-start.18 = (bf16[272,512]{1,0:T(8,128)(2,1)}, bf16[272,512]{1,0:T(8,128)(2,1)S(1)}, u32[]{:S(2)}) copy-start(bf16[272,512]{1,0:T(8,128)(2,1)S(1)} %collective-permute-done.32.refs_4_) | copy-start | bytes 835588
  83.1 34.3 %collective-permute-start.34 = (bf16[4,144,512]{2,1,0:T(8,128)(2,1)S(1)}, bf16[4,144,512]{2,1,0:T(8,128)(2,1)S(1)}, u32[]{:S(2)}, u32[]{:S(2)}) collective-permute-start(bf16[4,144,512]{2,1,0:T(8,128)(2,1)S(1)} %pad_maximum_fusion.refs_0_), channel_id=1, source_target_pairs={{0,1},{1,0},{2,3},{3,2},{4,5},{5,4},{6,7},{7,6},{8,9},{9,8},{10,11... | collective-permute-start | bytes 1769480 | tf_op jit(solution)/shard_map/ppermute | solution.py:477
  84.8 54.3 %copy-start.7 = (bf16[192,512]{1,0:T(8,128)(2,1)}, bf16[192,512]{1,0:T(8,128)(2,1)S(1)}, u32[]{:S(2)}) copy-start(bf16[192,512]{1,0:T(8,128)(2,1)S(1)} %add_convert_fusion.refs_3_.refs_5_) | copy-start | bytes 589828
  84.8 8.2 %collective-permute-start.15 = (bf16[192,512]{1,0:T(8,128)(2,1)S(1)}, bf16[192,512]{1,0:T(8,128)(2,1)S(1)}, u32[]{:S(2)}, u32[]{:S(2)}) collective-permute-start(bf16[192,512]{1,0:T(8,128)(2,1)S(1)} %add_convert_fusion.refs_3_.refs_5_), channel_id=1, source_target_pairs={{0,24},{8,0},{16,8},{24,16},{1,25},{9,1},{17,9},{25,17},{2,26},{10... | collective-permute-start | bytes 589832 | tf_op jit(solution)/shard_map/ppermute | solution.py:352
  87.6 19.0 %collective-permute-start.14 = (bf16[192,512]{1,0:T(8,128)(2,1)S(1)}, bf16[192,512]{1,0:T(8,128)(2,1)S(1)}, u32[]{:S(2)}, u32[]{:S(2)}) collective-permute-start(bf16[192,512]{1,0:T(8,128)(2,1)S(1)} %add_convert_fusion.refs_3_.refs_5_), channel_id=1, source_target_pairs={{0,16},{8,24},{16,0},{24,8},{1,17},{9,25},{17,1},{25,9},{2,18},{10... | collective-permute-start | bytes 589832 | tf_op jit(solution)/shard_map/ppermute | solution.py:352
  88.5 19.5 %collective-permute-start.13 = (bf16[192,512]{1,0:T(8,128)(2,1)S(1)}, bf16[192,512]{1,0:T(8,128)(2,1)S(1)}, u32[]{:S(2)}, u32[]{:S(2)}) collective-permute-start(bf16[192,512]{1,0:T(8,128)(2,1)S(1)} %add_convert_fusion.refs_3_.refs_5_), channel_id=1, source_target_pairs={{0,8},{8,16},{16,24},{24,0},{1,9},{9,17},{17,25},{25,1},{2,10},{10... | collective-permute-start | bytes 589832 | tf_op jit(solution)/shard_map/ppermute | solution.py:352
  90.5 24.9 %collective-permute-start.12 = (bf16[192,512]{1,0:T(8,128)(2,1)S(1)}, bf16[192,512]{1,0:T(8,128)(2,1)S(1)}, u32[]{:S(2)}, u32[]{:S(2)}) collective-permute-start(bf16[192,512]{1,0:T(8,128)(2,1)S(1)} %add_convert_fusion.refs_3_.refs_5_), channel_id=1, source_target_pairs={{0,6},{2,4},{4,2},{6,0},{1,7},{3,5},{5,3},{7,1},{8,14},{10,12},{12... | collective-permute-start | bytes 589832 | tf_op jit(solution)/shard_map/ppermute | solution.py:356
  93.0 23.8 %collective-permute-start.11 = (bf16[192,512]{1,0:T(8,128)(2,1)S(1)}, bf16[192,512]{1,0:T(8,128)(2,1)S(1)}, u32[]{:S(2)}, u32[]{:S(2)}) collective-permute-start(bf16[192,512]{1,0:T(8,128)(2,1)S(1)} %add_convert_fusion.refs_3_.refs_5_), channel_id=1, source_target_pairs={{0,4},{2,6},{4,0},{6,2},{1,5},{3,7},{5,1},{7,3},{8,12},{10,14},{12... | collective-permute-start | bytes 589832 | tf_op jit(solution)/shard_map/ppermute | solution.py:356
  106.6 7.3 %collective-permute-start.33 = (bf16[256,256]{1,0:T(8,128)(2,1)S(1)}, bf16[256,256]{1,0:T(8,128)(2,1)S(1)}, u32[]{:S(2)}, u32[]{:S(2)}) collective-permute-start(bf16[256,256]{1,0:T(8,128)(2,1)S(1)} %get-tuple-element.38.refs_0_.a_ref), channel_id=1, source_target_pairs={{0,6},{2,4},{4,2},{6,0},{1,7},{3,5},{5,3},{7,1},{8,14},{10,12},{12... | collective-permute-start | bytes 393224 | tf_op jit(solution)/shard_map/ppermute | solution.py:425
  108.1 31.6 %collective-permute-start.10 = (bf16[192,512]{1,0:T(8,128)(2,1)S(1)}, bf16[192,512]{1,0:T(8,128)(2,1)S(1)}, u32[]{:S(2)}, u32[]{:S(2)}) collective-permute-start(bf16[192,512]{1,0:T(8,128)(2,1)S(1)} %add_convert_fusion.refs_3_.refs_5_), channel_id=1, source_target_pairs={{0,2},{2,0},{4,6},{6,4},{1,3},{3,1},{5,7},{7,5},{8,10},{10,8},{12,... | collective-permute-start | bytes 589832 | tf_op jit(solution)/shard_map/ppermute | solution.py:356
  109.2 29.9 %copy-start.8 = (bf16[576,512]{1,0:T(8,128)(2,1)}, bf16[576,512]{1,0:T(8,128)(2,1)S(1)}, u32[]{:S(2)}) copy-start(bf16[576,512]{1,0:T(8,128)(2,1)S(1)} %shard_map.137.refs_9_) | copy-start | bytes 1769476
  113.9 33.7 %collective-permute-start.18 = (bf16[576,512]{1,0:T(8,128)(2,1)S(1)}, bf16[576,512]{1,0:T(8,128)(2,1)S(1)}, u32[]{:S(2)}, u32[]{:S(2)}) collective-permute-start(bf16[576,512]{1,0:T(8,128)(2,1)S(1)} %shard_map.137.refs_9_), channel_id=1, source_target_pairs={{0,6},{2,4},{4,2},{6,0},{1,7},{3,5},{5,3},{7,1},{8,14},{10,12},{12... | collective-permute-start | bytes 1769480 | tf_op jit(solution)/shard_map/ppermute | solution.py:356
  115.3 23.8 %copy-start.23 = (bf16[192,512]{1,0:T(8,128)(2,1)}, bf16[192,512]{1,0:T(8,128)(2,1)S(1)}, u32[]{:S(2)}) copy-start(bf16[192,512]{1,0:T(8,128)(2,1)S(1)} %collective-permute-done.12.refs_8_) | copy-start | bytes 589828
  115.3 32.3 %collective-permute-start.17 = (bf16[576,512]{1,0:T(8,128)(2,1)S(1)}, bf16[576,512]{1,0:T(8,128)(2,1)S(1)}, u32[]{:S(2)}, u32[]{:S(2)}) collective-permute-start(bf16[576,512]{1,0:T(8,128)(2,1)S(1)} %shard_map.137.refs_9_), channel_id=1, source_target_pairs={{0,4},{2,6},{4,0},{6,2},{1,5},{3,7},{5,1},{7,3},{8,12},{10,14},{12... | collective-permute-start | bytes 1769480 | tf_op jit(solution)/shard_map/ppermute | solution.py:356
  116.9 22.3 %copy-start.24 = (bf16[192,512]{1,0:T(8,128)(2,1)}, bf16[192,512]{1,0:T(8,128)(2,1)S(1)}, u32[]{:S(2)}) copy-start(bf16[192,512]{1,0:T(8,128)(2,1)S(1)} %collective-permute-done.11.refs_7_) | copy-start | bytes 589828
  116.9 30.8 %collective-permute-start.16 = (bf16[576,512]{1,0:T(8,128)(2,1)S(1)}, bf16[576,512]{1,0:T(8,128)(2,1)S(1)}, u32[]{:S(2)}, u32[]{:S(2)}) collective-permute-start(bf16[576,512]{1,0:T(8,128)(2,1)S(1)} %shard_map.137.refs_9_), channel_id=1, source_target_pairs={{0,2},{2,0},{4,6},{6,4},{1,3},{3,1},{5,7},{7,5},{8,10},{10,8},{12,... | collective-permute-start | bytes 1769480 | tf_op jit(solution)/shard_map/ppermute | solution.py:356
  117.4 30.2 %collective-permute-start.31 = (bf16[256,512]{1,0:T(8,128)(2,1)S(1)}, bf16[256,512]{1,0:T(8,128)(2,1)S(1)}, u32[]{:S(2)}, u32[]{:S(2)}) collective-permute-start(bf16[256,512]{1,0:T(8,128)(2,1)S(1)} %slice.34), channel_id=1, source_target_pairs={{0,2},{2,0},{4,6},{6,4},{1,3},{3,1},{5,7},{7,5},{8,10},{10,8},{12,... | collective-permute-start | bytes 786440 | tf_op jit(solution)/shard_map/ppermute | solution.py:387
  139.7 108.3 %copy-start.4 = (bf16[704,512]{1,0:T(8,128)(2,1)S(1)}, bf16[704,512]{1,0:T(8,128)(2,1)}, u32[]{:S(2)}) copy-start(bf16[704,512]{1,0:T(8,128)(2,1)} %copy-done.3) | copy-start | bytes 2162692
  139.7 108.3 %copy-start.6 = (bf16[704,512]{1,0:T(8,128)(2,1)S(1)}, bf16[704,512]{1,0:T(8,128)(2,1)}, u32[]{:S(2)}) copy-start(bf16[704,512]{1,0:T(8,128)(2,1)} %copy-done.5) | copy-start | bytes 2162692
  139.7 7.9 %copy-start.25 = (bf16[192,512]{1,0:T(8,128)(2,1)}, bf16[192,512]{1,0:T(8,128)(2,1)S(1)}, u32[]{:S(2)}) copy-start(bf16[192,512]{1,0:T(8,128)(2,1)S(1)} %collective-permute-done.10.refs_6_) | copy-start | bytes 589828
  147.6 3.0 %copy-start.22 = (bf16[256,512]{1,0:T(8,128)(2,1)}, bf16[256,512]{1,0:T(8,128)(2,1)S(1)}, u32[]{:S(2)}) copy-start(bf16[256,512]{1,0:T(8,128)(2,1)S(1)} %collective-permute-done.31.refs_3_) | copy-start | bytes 786436
  147.6 3.0 %copy-start.19 = (bf16[576,512]{1,0:T(8,128)(2,1)}, bf16[576,512]{1,0:T(8,128)(2,1)S(1)}, u32[]{:S(2)}) copy-start(bf16[576,512]{1,0:T(8,128)(2,1)S(1)} %collective-permute-done.18.refs_12_) | copy-start | bytes 1769476
  147.6 3.0 %copy-start.20 = (bf16[576,512]{1,0:T(8,128)(2,1)}, bf16[576,512]{1,0:T(8,128)(2,1)S(1)}, u32[]{:S(2)}) copy-start(bf16[576,512]{1,0:T(8,128)(2,1)S(1)} %collective-permute-done.17.refs_11_) | copy-start | bytes 1769476
  147.6 3.0 %copy-start.21 = (bf16[576,512]{1,0:T(8,128)(2,1)}, bf16[576,512]{1,0:T(8,128)(2,1)S(1)}, u32[]{:S(2)}) copy-start(bf16[576,512]{1,0:T(8,128)(2,1)S(1)} %collective-permute-done.16.refs_10_) | copy-start | bytes 1769476
  147.6 104.6 %collective-permute-start.35 = (bf16[704,512]{1,0:T(8,128)(2,1)S(1)}, bf16[704,512]{1,0:T(8,128)(2,1)S(1)}, u32[]{:S(2)}, u32[]{:S(2)}) collective-permute-start(bf16[704,512]{1,0:T(8,128)(2,1)S(1)} %broadcast_select_fusion.1.refs_0_.a_ref), channel_id=1, source_target_pairs={{0,6},{2,4},{4,2},{6,0},{1,7},{3,5},{5,3},{7,1},{8,14},{10,12},{12... | collective-permute-start | bytes 2162696 | tf_op jit(solution)/shard_map/ppermute | solution.py:503
  149.6 98.3 %collective-permute-start.36 = (bf16[704,512]{1,0:T(8,128)(2,1)S(1)}, bf16[704,512]{1,0:T(8,128)(2,1)S(1)}, u32[]{:S(2)}, u32[]{:S(2)}) collective-permute-start(bf16[704,512]{1,0:T(8,128)(2,1)S(1)} %collective-permute-done.2.refs_1_.a_ref), channel_id=1, source_target_pairs={{0,6},{2,4},{4,2},{6,0},{1,7},{3,5},{5,3},{7,1},{8,14},{10,12},{12... | collective-permute-start | bytes 2162696 | tf_op jit(solution)/shard_map/ppermute | solution.py:502
  248.0 1.6 copy-start
  249.6 1.9 copy-start.16
  249.6 2.7 %copy-start.2 = (bf16[704,512]{1,0:T(8,128)(2,1)S(1)}, bf16[704,512]{1,0:T(8,128)(2,1)}, u32[]{:S(2)}) copy-start(bf16[704,512]{1,0:T(8,128)(2,1)} %copy-done.1) | copy-start | bytes 2162692
  251.4 2.7 %collective-permute-start.37 = (bf16[704,512]{1,0:T(8,128)(2,1)S(1)}, bf16[704,512]{1,0:T(8,128)(2,1)S(1)}, u32[]{:S(2)}, u32[]{:S(2)}) collective-permute-start(bf16[704,512]{1,0:T(8,128)(2,1)S(1)} %shard_map.146), channel_id=1, source_target_pairs={{0,1},{1,0},{2,3},{3,2},{4,5},{5,4},{6,7},{7,6},{8,9},{9,8},{10,11... | collective-permute-start | bytes 2162696 | tf_op jit(solution)/shard_map/ppermute | solution.py:505
  252.2 1.9 copy-start.12
  252.2 1.9 copy-start.13

commit v2 on v1

--- a/solution.py
+++ b/solution.py
@@ -243,14 +243,18 @@
     out_ref[...] = total.astype(BF16)
 
 
-def apply(blocks, q):
+def apply(blocks, q, skip=0):
     rows, nb = blocks[0].shape
     step = rows // 2 if rows % 32 == 0 else rows
     block = pl.BlockSpec((step, nb), lambda i: (i, 0))
     return pl.pallas_call(
         apply_kernel,
         grid=(rows // step,),
-        in_specs=[block] * 4 + [pl.BlockSpec((4 * nb, nb), lambda i: (0, 0))],
+        in_specs=[block] * 3
+        + [
+            pl.BlockSpec((step, nb), lambda i: (i + skip * rows // step, 0)),
+            pl.BlockSpec((4 * nb, nb), lambda i: (0, 0)),
+        ],
         out_specs=block,
         out_shape=jax.ShapeDtypeStruct((rows, nb), BF16),
         compiler_params=pltpu.CompilerParams(vmem_limit_bytes=16 * 2**20),
@@ -479,8 +483,9 @@
     small_q = chain(None, [spreads, others], place, f_size, n)
     small_out = apply([small, small_x, small_y, small_d], small_q)
 
-    own_groups, rest_groups, first_groups, small_out, keep, gift = lax.optimization_barrier(
-        (own_groups, rest_groups, first_groups, small_out, keep, gift)
+    both = jnp.concatenate([keep, gift], axis=0)
+    own_groups, rest_groups, first_groups, small_out, both = lax.optimization_barrier(
+        (own_groups, rest_groups, first_groups, small_out, both)
     )
     n = 4 * nb
     plan = []
@@ -499,11 +504,10 @@
             plan.append((b, 9 + b, (step - 1) * height, height, base, height, step))
     both_q = chain(plan, [*first_groups, *own_groups, *rest_groups], place, f_size, n)
 
-    gift_d = lax.ppermute(gift, "tp", swap(4, 3))
-    keep_d = lax.ppermute(keep, "tp", swap(4, 3))
-    sent = apply([gift, gift_x, gift_y, gift_d], both_q)
+    both_d = lax.ppermute(both, "tp", swap(4, 3))
+    sent = apply([gift, gift_x, gift_y, both_d], both_q, 1)
     arrived = lax.ppermute(sent, "rep", cross)
-    kept = apply([keep, keep_x, keep_y, keep_d], both_q)
+    kept = apply([keep, keep_x, keep_y, both_d], both_q)
     finals = (
         jnp.where(rep == 0, kept, arrived),
         jnp.where(rep == 0, arrived, kept),

time: 257 us -> 252 us (0.981)
  waiting for transfers between devices: 60.1 us -> 51.3 us
    ppermute x6, waiting for transfers between devices: 0.02 us -> 6.65 us  [around(): return [value] + [lax.ppermute(value, 'tp', swap(4, b)) for b in (1, 2, 3)]]
    ppermute x6, waiting for transfers between devices: 15 us -> 9.12 us  [spread(): lax.ppermute(piece, 'fs', shift(size, step))]
    ppermute x1, waiting for transfers between devices: 4.62 us -> 0.01 us  [update(): small_d = lax.ppermute(small, 'tp', swap(4, 3))]
    ppermute x1, waiting for transfers between devices: 4.56 us -> 0.03 us  [update(): gift_y = lax.ppermute(gift, 'tp', swap(4, 2))]
    ppermute x1, waiting for transfers between devices: 7.87 us -> 3.63 us  [relay(): upper = lax.ppermute(upper, 'tp', swap(4, 1))]
    ppermute x1, waiting for transfers between devices: 0.01 us -> 3.38 us  [update(): gift_x = lax.ppermute(gift, 'tp', swap(4, 1))]
  transfers between devices with their start and end apart: 38 -> 37, of which waited for: 15 -> 14; matrix products, arithmetic and copies ran while one was open for 5% -> 5% of each run, Pallas kernels for 49% -> 50%
where the time goes in v2:
time: 252 us; the launch traced here: 251 us
  Pallas kernels  127 us (50%)
  waiting for transfers between devices  51.3 us (20%)
  starting transfers between devices  49.8 us (20%)
  local copies, waits for them, and re-layouts  12.3 us (5%)
  other arithmetic  9.47 us (4%)
    pallas_call x2, Pallas kernels, chain(): pl.pallas_call(functools.partial(chain_kernel, plan, size, tile), out_sha...  117 us
    ppermute x6, waiting for transfers between devices, scatter(): lax.ppermute(chunk(lax.rem(place + step, size)), 'fs', shift(size, step))  15.5 us
    ppermute x6, starting transfers between devices, spread(): lax.ppermute(piece, 'fs', shift(size, step))  10.5 us
    ppermute x6, starting transfers between devices, scatter(): lax.ppermute(chunk(lax.rem(place + step, size)), 'fs', shift(size, step))  10.1 us
    ppermute x6, starting transfers between devices, around(): return [value] + [lax.ppermute(value, 'tp', swap(4, b)) for b in (1, 2, 3)]  9.76 us
    ppermute x6, waiting for transfers between devices, spread(): lax.ppermute(piece, 'fs', shift(size, step))  9.12 us
    ppermute x6, waiting for transfers between devices, around(): return [value] + [lax.ppermute(value, 'tp', swap(4, b)) for b in (1, 2, 3)]  6.65 us
    convert_element_type x3, local copies, waits for them, and re-layouts, half_sum(): return (mine, theirs.astype(BF16))  5.78 us
  transfers between devices with their start and end apart: 37, of which 14 were waited for; matrix products, arithmetic and copies ran while one was open for 5% of the time, Pallas kernels for 50%

profile of v2, /device:TPU:0, one launch (start us, length us, event | category | flops | bytes accessed | tf_op | source)
XLA Modules:
  0.0 250.9 jit_solution(11388014885414286595)
XLA Ops:
  0.6 2.4 fusion.2
  3.0 0.5 collective-permute-start
  3.5 2.5 fusion.3
  6.0 1.0 fusion.7
  6.9 0.6 collective-permute-start.19
  7.5 1.0 collective-permute-done.19
  8.6 1.7 fusion.12
  10.3 2.8 %collective-permute-start.20 = (bf16[256,256]{1,0:T(8,128)(2,1)S(1)}, bf16[256,256]{1,0:T(8,128)(2,1)S(1)}, u32[]{:S(2)}, u32[]{:S(2)}) collective-permute-start(bf16[256,256]{1,0:T(8,128)(2,1)S(1)} %get-tuple-element.36.refs_0_.a_ref), channel_id=1, source_target_pairs={{0,2},{2,0},{4,6},{6,4},{1,3},{3,1},{5,7},{7,5},{8,10},{10,8},{12,... | collective-permute-start | bytes 393224 | tf_op jit(solution)/shard_map/ppermute | solution.py:427
  13.0 1.5 collective-permute-start.21
  14.9 2.0 collective-permute-done.20.refs_1_.b_ref
  16.9 1.5 collective-permute-done.21.refs_2_.c_ref
  18.4 1.0 shard_map.140
  19.7 3.5 %broadcast_select_fusion = (bf16[704,512]{1,0:T(8,128)(2,1)S(1)}, f32[704,512]{1,0:T(8,128)S(1)}, f32[704,512]{1,0:T(8,128)S(1)}) fusion(pred[]{:T(512)S(6)} %eq.2, bf16[704,512]{1,0:T(8,128)(2,1)} %collective-permute-done.1, f32[1,1408,512]{2,1,0:T(8,128)S(1)} %copy-done.12, s32[]{:T(128)S(6)} %select_n.76, f32[704,512]{1,0:T(8,128)} %param.13, ...), kind=kLoop, calls=%fused_computation.11 | loop fusion | flops 3964928 | bytes 10813445 | tf_op jit(solution)/shard_map/jit(_where)/select_n | solution.py:426
  23.2 0.5 collective-permute-start.4
  25.1 1.7 collective-permute-start.3
  26.9 1.0 shard_map.138
  27.9 1.6 collective-permute-start.5
  29.5 0.5 collective-permute-start.6
  30.0 1.6 collective-permute-start.23
  31.6 5.3 %collective-permute-done.23 = bf16[132,512]{1,0:T(8,128)(2,1)S(1)} collective-permute-done((bf16[132,512]{1,0:T(8,128)(2,1)S(1)}, bf16[132,512]{1,0:T(8,128)(2,1)S(1)}, u32[]{:S(2)}, u32[]{:S(2)}) %collective-permute-start.23) | collective-permute-done | bytes 135200 | tf_op jit(solution)/shard_map/ppermute | solution.py:343
  36.9 0.8 collective-permute-start.24
  37.7 6.4 %collective-permute-done.24 = bf16[132,512]{1,0:T(8,128)(2,1)S(1)} collective-permute-done((bf16[132,512]{1,0:T(8,128)(2,1)S(1)}, bf16[132,512]{1,0:T(8,128)(2,1)S(1)}, u32[]{:S(2)}, u32[]{:S(2)}) %collective-permute-start.24) | collective-permute-done | bytes 135200 | tf_op jit(solution)/shard_map/ppermute | solution.py:343
  44.1 2.5 collective-permute-start.25
  46.5 3.8 %collective-permute-done.25 = bf16[132,512]{1,0:T(8,128)(2,1)S(1)} collective-permute-done((bf16[132,512]{1,0:T(8,128)(2,1)S(1)}, bf16[132,512]{1,0:T(8,128)(2,1)S(1)}, u32[]{:S(2)}, u32[]{:S(2)}) %collective-permute-start.25) | collective-permute-done | bytes 135200 | tf_op jit(solution)/shard_map/ppermute | solution.py:343
  50.5 4.8 %collective-permute-start.27 = (bf16[132,512]{1,0:T(8,128)(2,1)S(1)}, bf16[132,512]{1,0:T(8,128)(2,1)S(1)}, u32[]{:S(2)}, u32[]{:S(2)}) collective-permute-start(bf16[132,512]{1,0:T(8,128)(2,1)S(1)} %add_convert_fusion.2.refs_0_), channel_id=1, source_target_pairs={{0,16},{8,24},{16,0},{24,8},{1,17},{9,25},{17,1},{25,9},{2,18},{10... | collective-permute-start | bytes 405512 | tf_op jit(solution)/shard_map/ppermute | solution.py:356
  55.4 3.4 %collective-permute-done.5.refs_3_.b_ref = bf16[704,512]{1,0:T(8,128)(2,1)S(1)} collective-permute-done((bf16[704,512]{1,0:T(8,128)(2,1)S(1)}, bf16[704,512]{1,0:T(8,128)(2,1)S(1)}, u32[]{:S(2)}, u32[]{:S(2)}) %collective-permute-start.5) | collective-permute-done | bytes 720928 | tf_op jit(solution)/shard_map/ppermute | solution.py:433
  58.8 2.2 shard_map.136.refs_4_
  61.0 1.6 collective-permute-done.27.refs_2_
  62.6 0.8 shard_map.141.refs_0_
  63.4 0.7 collective-permute-start.29
  64.1 1.4 collective-permute-start.30
  65.5 2.3 collective-permute-start.7
  67.8 1.5 collective-permute-start.8
  69.4 1.3 collective-permute-start.9
  70.7 0.9 slice_bitcast_fusion.3
  71.6 4.3 %collective-permute-done.29.refs_1_ = bf16[528,512]{1,0:T(8,128)(2,1)} collective-permute-done((bf16[528,512]{1,0:T(8,128)(2,1)}, bf16[528,512]{1,0:T(8,128)(2,1)}, u32[]{:S(2)}, u32[]{:S(2)}) %collective-permute-start.29) | collective-permute-done | bytes 540704 | tf_op jit(solution)/shard_map/ppermute | solution.py:388
  76.0 1.0 slice.35
  76.9 1.6 collective-permute-start.32
  78.5 0.9 slice_bitcast_fusion.2
  79.5 4.1 %collective-permute-done.32.refs_4_ = bf16[272,512]{1,0:T(8,128)(2,1)S(1)} collective-permute-done((bf16[272,512]{1,0:T(8,128)(2,1)S(1)}, bf16[272,512]{1,0:T(8,128)(2,1)S(1)}, u32[]{:S(2)}, u32[]{:S(2)}) %collective-permute-start.32) | collective-permute-done | bytes 278560 | tf_op jit(solution)/shard_map/ppermute | solution.py:392
  83.6 0.7 copy-done.18
  84.6 3.1 %collective-permute-start.13 = (bf16[192,512]{1,0:T(8,128)(2,1)S(1)}, bf16[192,512]{1,0:T(8,128)(2,1)S(1)}, u32[]{:S(2)}, u32[]{:S(2)}) collective-permute-start(bf16[192,512]{1,0:T(8,128)(2,1)S(1)} %add_convert_fusion.refs_3_.refs_5_), channel_id=1, source_target_pairs={{0,8},{8,16},{16,24},{24,0},{1,9},{9,17},{17,25},{25,1},{2,10},{10... | collective-permute-start | bytes 589832 | tf_op jit(solution)/shard_map/ppermute | solution.py:356
  87.7 1.2 collective-permute-start.14
  88.9 2.9 %collective-permute-start.33 = (bf16[256,256]{1,0:T(8,128)(2,1)S(1)}, bf16[256,256]{1,0:T(8,128)(2,1)S(1)}, u32[]{:S(2)}, u32[]{:S(2)}) collective-permute-start(bf16[256,256]{1,0:T(8,128)(2,1)S(1)} %get-tuple-element.36.refs_0_.a_ref), channel_id=1, source_target_pairs={{0,6},{2,4},{4,2},{6,0},{1,7},{3,5},{5,3},{7,1},{8,14},{10,12},{12... | collective-permute-start | bytes 393224 | tf_op jit(solution)/shard_map/ppermute | solution.py:429
  91.7 1.3 collective-permute-start.15
  93.1 1.2 collective-permute-done.13.refs_0_
  94.3 1.8 collective-permute-start.10
  96.1 6.3 %collective-permute-done.14.refs_1_ = bf16[192,512]{1,0:T(8,128)(2,1)S(1)} collective-permute-done((bf16[192,512]{1,0:T(8,128)(2,1)S(1)}, bf16[192,512]{1,0:T(8,128)(2,1)S(1)}, u32[]{:S(2)}, u32[]{:S(2)}) %collective-permute-start.14) | collective-permute-done | bytes 196640 | tf_op jit(solution)/shard_map/ppermute | solution.py:356
  102.4 1.5 collective-permute-start.11
  104.0 2.0 collective-permute-start.12
  106.2 1.5 collective-permute-start.17
  107.7 6.6 %collective-permute-done.11.refs_7_ = bf16[192,512]{1,0:T(8,128)(2,1)S(1)} collective-permute-done((bf16[192,512]{1,0:T(8,128)(2,1)S(1)}, bf16[192,512]{1,0:T(8,128)(2,1)S(1)}, u32[]{:S(2)}, u32[]{:S(2)}) %collective-permute-start.11) | collective-permute-done | bytes 196640 | tf_op jit(solution)/shard_map/ppermute | solution.py:360
  114.4 2.9 %collective-permute-start.18 = (bf16[576,512]{1,0:T(8,128)(2,1)S(1)}, bf16[576,512]{1,0:T(8,128)(2,1)}, u32[]{:S(2)}, u32[]{:S(2)}) collective-permute-start(bf16[576,512]{1,0:T(8,128)(2,1)S(1)} %shard_map.137.refs_9_), channel_id=1, source_target_pairs={{0,6},{2,4},{4,2},{6,0},{1,7},{3,5},{5,3},{7,1},{8,14},{10,12},{12... | collective-permute-start | bytes 1769480 | tf_op jit(solution)/shard_map/ppermute | solution.py:360
  117.3 20.2 %shard_map.142.q_ref = bf16[1024,256]{1,0:T(8,128)(2,1)S(1)} custom-call(s32[3]{0:T(128)S(1)} %pad_add_fusion.place_ref, bf16[4,144,512]{2,1,0:T(8,128)(2,1)S(1)} %pad_maximum_fusion.1.refs_0_, bf16[4,144,512]{2,1,0:T(8,128)(2,1)S(1)} %collective-permute-done.34.refs_1_), custom_call_target="tpu_custom_call" | custom-call | flops 10737418240 | bytes 1572864 | tf_op jit(solution)/shard_map/pallas_call | solution.py:218
  137.6 0.5 shard_map.143
  138.1 3.6 %collective-permute-done.31.refs_3_ = bf16[256,512]{1,0:T(8,128)(2,1)S(1)} collective-permute-done((bf16[256,512]{1,0:T(8,128)(2,1)S(1)}, bf16[256,512]{1,0:T(8,128)(2,1)S(1)}, u32[]{:S(2)}, u32[]{:S(2)}) %collective-permute-start.31) | collective-permute-done | bytes 262176 | tf_op jit(solution)/shard_map/ppermute | solution.py:391
  141.8 0.9 copy-done.20
  142.7 2.6 %collective-permute-start.35 = (bf16[1408,512]{1,0:T(8,128)(2,1)S(1)}, bf16[1408,512]{1,0:T(8,128)(2,1)S(1)}, u32[]{:S(2)}, u32[]{:S(2)}) collective-permute-start(bf16[1408,512]{1,0:T(8,128)(2,1)S(1)} %pad_maximum_fusion), channel_id=1, source_target_pairs={{0,6},{2,4},{4,2},{6,0},{1,7},{3,5},{5,3},{7,1},{8,14},{10,12},{12... | collective-permute-start | bytes 4325384 | tf_op jit(solution)/shard_map/ppermute | solution.py:507
  145.3 97.3 %shard_map.144.q_ref = bf16[2048,512]{1,0:T(8,128)(2,1)} custom-call(s32[3]{0:T(128)} %copy-done.9, bf16[528,512]{1,0:T(8,128)(2,1)} %shard_map.141.refs_0_, bf16[528,512]{1,0:T(8,128)(2,1)} %collective-permute-done.29.refs_1_, bf16[528,512]{1,0:T(8,128)(2,1)} %copy-done.15, bf16[256,512]{1,0:T(8,128)(2,1)} %copy-done.21, bf16[272,512]{1,0:T(8,128)(2,1)} %copy-done.18, ...), custom_call_target="tpu_custom_call" | custom-call | flops 85899345920 | bytes 6291456 | tf_op jit(solution)/shard_map/pallas_call | solution.py:218
  242.6 1.6 copy-done
  244.2 1.8 shard_map.146
  246.1 0.7 multiply_subtract_fusion.2
  246.9 1.8 shard_map.145
  248.7 2.2 multiply_subtract_fusion
  (99 shorter events, 3.1 us)
Async XLA Ops:
  0.6 7.9 %copy-start.17 = (f32[256,256]{1,0:T(8,128)S(1)}, f32[256,256]{1,0:T(8,128)}, u32[]{:S(2)}) copy-start(f32[256,256]{1,0:T(8,128)} %param.16) | copy-start | bytes 786436
  3.0 16.6 %collective-permute-start = (bf16[704,512]{1,0:T(8,128)(2,1)}, bf16[704,512]{1,0:T(8,128)(2,1)}, u32[]{:S(2)}, u32[]{:S(2)}) collective-permute-start(bf16[704,512]{1,0:T(8,128)(2,1)} %fusion.2), channel_id=1, source_target_pairs={{0,1},{1,0},{2,3},{3,2},{4,5},{5,4},{6,7},{7,6},{8,9},{9,8},{10,11... | collective-permute-start | bytes 2162696 | tf_op jit(solution)/shard_map/ppermute | solution.py:418
  3.5 16.2 %copy-start.12 = (f32[1,1408,512]{2,1,0:T(8,128)S(1)}, f32[1,1408,512]{2,1,0:T(8,128)}, u32[]{:S(2)}) copy-start(f32[1,1408,512]{2,1,0:T(8,128)} %param.12) | copy-start | bytes 8650756
  6.0 13.7 %collective-permute-start.1 = (bf16[704,512]{1,0:T(8,128)(2,1)}, bf16[704,512]{1,0:T(8,128)(2,1)}, u32[]{:S(2)}, u32[]{:S(2)}) collective-permute-start(bf16[704,512]{1,0:T(8,128)(2,1)} %fusion.3), channel_id=1, source_target_pairs={{0,1},{1,0},{2,3},{3,2},{4,5},{5,4},{6,7},{7,6},{8,9},{9,8},{10,11... | collective-permute-start | bytes 2162696 | tf_op jit(solution)/shard_map/ppermute | solution.py:418
  6.9 1.6 collective-permute-start.19
  10.3 6.6 %collective-permute-start.20 = (bf16[256,256]{1,0:T(8,128)(2,1)S(1)}, bf16[256,256]{1,0:T(8,128)(2,1)S(1)}, u32[]{:S(2)}, u32[]{:S(2)}) collective-permute-start(bf16[256,256]{1,0:T(8,128)(2,1)S(1)} %get-tuple-element.36.refs_0_.a_ref), channel_id=1, source_target_pairs={{0,2},{2,0},{4,6},{6,4},{1,3},{3,1},{5,7},{7,5},{8,10},{10,8},{12,... | collective-permute-start | bytes 393224 | tf_op jit(solution)/shard_map/ppermute | solution.py:427
  13.0 5.3 %collective-permute-start.21 = (bf16[256,256]{1,0:T(8,128)(2,1)S(1)}, bf16[256,256]{1,0:T(8,128)(2,1)S(1)}, u32[]{:S(2)}, u32[]{:S(2)}) collective-permute-start(bf16[256,256]{1,0:T(8,128)(2,1)S(1)} %get-tuple-element.36.refs_0_.a_ref), channel_id=1, source_target_pairs={{0,4},{2,6},{4,0},{6,2},{1,5},{3,7},{5,1},{7,3},{8,12},{10,14},{12... | collective-permute-start | bytes 393224 | tf_op jit(solution)/shard_map/ppermute | solution.py:428
  14.6 102.7 %copy-start.9 = (s32[3]{0:T(128)}, s32[3]{0:T(128)S(1)}, u32[]{:S(2)}) copy-start(s32[3]{0:T(128)S(1)} %pad_add_fusion.place_ref) | copy-start | bytes 40
  19.6 4.2 %collective-permute-start.22 = (bf16[288,256]{1,0:T(8,128)(2,1)S(1)}, bf16[288,256]{1,0:T(8,128)(2,1)S(1)}, u32[]{:S(2)}, u32[]{:S(2)}) collective-permute-start(bf16[288,256]{1,0:T(8,128)(2,1)S(1)} %fusion.5), channel_id=1, source_target_pairs={{0,1},{1,0},{2,3},{3,2},{4,5},{5,4},{6,7},{7,6},{8,9},{9,8},{10,11... | collective-permute-start | bytes 442376 | tf_op jit(solution)/shard_map/ppermute | solution.py:443
  23.2 1.3 copy-start.10
  23.2 1.6 copy-start.11
  23.2 3.6 %collective-permute-start.4 = (bf16[704,512]{1,0:T(8,128)(2,1)S(1)}, bf16[704,512]{1,0:T(8,128)(2,1)S(1)}, u32[]{:S(2)}, u32[]{:S(2)}) collective-permute-start(bf16[704,512]{1,0:T(8,128)(2,1)S(1)} %get-tuple-element.38), channel_id=1, source_target_pairs={{0,1},{1,0},{2,3},{3,2},{4,5},{5,4},{6,7},{7,6},{8,9},{9,8},{10,11... | collective-permute-start | bytes 2162696 | tf_op jit(solution)/shard_map/ppermute | solution.py:432
  24.8 25.7 %collective-permute-start.2 = (bf16[704,512]{1,0:T(8,128)(2,1)S(1)}, bf16[704,512]{1,0:T(8,128)(2,1)S(1)}, u32[]{:S(2)}, u32[]{:S(2)}) collective-permute-start(bf16[704,512]{1,0:T(8,128)(2,1)S(1)} %broadcast_select_fusion.1.refs_0_.a_ref), channel_id=1, source_target_pairs={{0,2},{2,0},{4,6},{6,4},{1,3},{3,1},{5,7},{7,5},{8,10},{10,8},{12,... | collective-permute-start | bytes 2162696 | tf_op jit(solution)/shard_map/ppermute | solution.py:430
  25.1 30.3 %collective-permute-start.3 = (bf16[704,512]{1,0:T(8,128)(2,1)S(1)}, bf16[704,512]{1,0:T(8,128)(2,1)S(1)}, u32[]{:S(2)}, u32[]{:S(2)}) collective-permute-start(bf16[704,512]{1,0:T(8,128)(2,1)S(1)} %broadcast_select_fusion.1.refs_0_.a_ref), channel_id=1, source_target_pairs={{0,4},{2,6},{4,0},{6,2},{1,5},{3,7},{5,1},{7,3},{8,12},{10,14},{12... | collective-permute-start | bytes 2162696 | tf_op jit(solution)/shard_map/ppermute | solution.py:431
  27.9 30.8 %collective-permute-start.5 = (bf16[704,512]{1,0:T(8,128)(2,1)S(1)}, bf16[704,512]{1,0:T(8,128)(2,1)S(1)}, u32[]{:S(2)}, u32[]{:S(2)}) collective-permute-start(bf16[704,512]{1,0:T(8,128)(2,1)S(1)} %collective-permute-done.4.refs_1_.a_ref), channel_id=1, source_target_pairs={{0,2},{2,0},{4,6},{6,4},{1,3},{3,1},{5,7},{7,5},{8,10},{10,8},{12,... | collective-permute-start | bytes 2162696 | tf_op jit(solution)/shard_map/ppermute | solution.py:433
  29.5 29.3 %collective-permute-start.6 = (bf16[704,512]{1,0:T(8,128)(2,1)S(1)}, bf16[704,512]{1,0:T(8,128)(2,1)S(1)}, u32[]{:S(2)}, u32[]{:S(2)}) collective-permute-start(bf16[704,512]{1,0:T(8,128)(2,1)S(1)} %collective-permute-done.4.refs_1_.a_ref), channel_id=1, source_target_pairs={{0,4},{2,6},{4,0},{6,2},{1,5},{3,7},{5,1},{7,3},{8,12},{10,14},{12... | collective-permute-start | bytes 2162696 | tf_op jit(solution)/shard_map/ppermute | solution.py:434
  30.0 6.9 %collective-permute-start.23 = (bf16[132,512]{1,0:T(8,128)(2,1)S(1)}, bf16[132,512]{1,0:T(8,128)(2,1)S(1)}, u32[]{:S(2)}, u32[]{:S(2)}) collective-permute-start(bf16[132,512]{1,0:T(8,128)(2,1)S(1)} %pad_maximum_fusion.2), channel_id=1, source_target_pairs={{0,8},{8,16},{16,24},{24,0},{1,9},{9,17},{17,25},{25,1},{2,10},{10... | collective-permute-start | bytes 405512 | tf_op jit(solution)/shard_map/ppermute | solution.py:343
  36.9 7.2 %collective-permute-start.24 = (bf16[132,512]{1,0:T(8,128)(2,1)S(1)}, bf16[132,512]{1,0:T(8,128)(2,1)S(1)}, u32[]{:S(2)}, u32[]{:S(2)}) collective-permute-start(bf16[132,512]{1,0:T(8,128)(2,1)S(1)} %pad_maximum_fusion.3), channel_id=1, source_target_pairs={{0,16},{8,24},{16,0},{24,8},{1,17},{9,25},{17,1},{25,9},{2,18},{10... | collective-permute-start | bytes 405512 | tf_op jit(solution)/shard_map/ppermute | solution.py:343
  44.1 6.3 %collective-permute-start.25 = (bf16[132,512]{1,0:T(8,128)(2,1)S(1)}, bf16[132,512]{1,0:T(8,128)(2,1)S(1)}, u32[]{:S(2)}, u32[]{:S(2)}) collective-permute-start(bf16[132,512]{1,0:T(8,128)(2,1)S(1)} %pad_maximum_fusion.4), channel_id=1, source_target_pairs={{0,24},{8,0},{16,8},{24,16},{1,25},{9,1},{17,9},{25,17},{2,26},{10... | collective-permute-start | bytes 405512 | tf_op jit(solution)/shard_map/ppermute | solution.py:343
  50.5 10.5 %collective-permute-start.26 = (bf16[132,512]{1,0:T(8,128)(2,1)S(1)}, bf16[132,512]{1,0:T(8,128)(2,1)S(1)}, u32[]{:S(2)}, u32[]{:S(2)}) collective-permute-start(bf16[132,512]{1,0:T(8,128)(2,1)S(1)} %add_convert_fusion.2.refs_0_), channel_id=1, source_target_pairs={{0,8},{8,16},{16,24},{24,0},{1,9},{9,17},{17,25},{25,1},{2,10},{10... | collective-permute-start | bytes 405512 | tf_op jit(solution)/shard_map/ppermute | solution.py:356
  50.5 12.0 %collective-permute-start.27 = (bf16[132,512]{1,0:T(8,128)(2,1)S(1)}, bf16[132,512]{1,0:T(8,128)(2,1)S(1)}, u32[]{:S(2)}, u32[]{:S(2)}) collective-permute-start(bf16[132,512]{1,0:T(8,128)(2,1)S(1)} %add_convert_fusion.2.refs_0_), channel_id=1, source_target_pairs={{0,16},{8,24},{16,0},{24,8},{1,17},{9,25},{17,1},{25,9},{2,18},{10... | collective-permute-start | bytes 405512 | tf_op jit(solution)/shard_map/ppermute | solution.py:356
  55.4 5.6 %copy-start.1 = (bf16[704,512]{1,0:T(8,128)(2,1)}, bf16[704,512]{1,0:T(8,128)(2,1)S(1)}, u32[]{:S(2)}) copy-start(bf16[704,512]{1,0:T(8,128)(2,1)S(1)} %collective-permute-done.3.refs_4_.c_ref) | copy-start | bytes 2162692
  55.4 7.2 %collective-permute-start.28 = (bf16[132,512]{1,0:T(8,128)(2,1)S(1)}, bf16[132,512]{1,0:T(8,128)(2,1)S(1)}, u32[]{:S(2)}, u32[]{:S(2)}) collective-permute-start(bf16[132,512]{1,0:T(8,128)(2,1)S(1)} %add_convert_fusion.2.refs_0_), channel_id=1, source_target_pairs={{0,24},{8,0},{16,8},{24,16},{1,25},{9,1},{17,9},{25,17},{2,26},{10... | collective-permute-start | bytes 405512 | tf_op jit(solution)/shard_map/ppermute | solution.py:356
  58.8 2.2 copy-start.3
  58.8 2.2 copy-start.5
  63.4 12.5 %collective-permute-start.29 = (bf16[528,512]{1,0:T(8,128)(2,1)}, bf16[528,512]{1,0:T(8,128)(2,1)}, u32[]{:S(2)}, u32[]{:S(2)}) collective-permute-start(bf16[528,512]{1,0:T(8,128)(2,1)} %shard_map.141.refs_0_), channel_id=1, source_target_pairs={{0,2},{2,0},{4,6},{6,4},{1,3},{3,1},{5,7},{7,5},{8,10},{10,8},{12,... | collective-permute-start | bytes 1622024 | tf_op jit(solution)/shard_map/ppermute | solution.py:388
  64.1 15.3 %collective-permute-start.30 = (bf16[528,512]{1,0:T(8,128)(2,1)}, bf16[528,512]{1,0:T(8,128)(2,1)S(1)}, u32[]{:S(2)}, u32[]{:S(2)}) collective-permute-start(bf16[528,512]{1,0:T(8,128)(2,1)} %shard_map.141.refs_0_), channel_id=1, source_target_pairs={{0,4},{2,6},{4,0},{6,2},{1,5},{3,7},{5,1},{7,3},{8,12},{10,14},{12... | collective-permute-start | bytes 1622024 | tf_op jit(solution)/shard_map/ppermute | solution.py:389
  65.5 18.9 %collective-permute-start.7 = (bf16[192,512]{1,0:T(8,128)(2,1)S(1)}, bf16[192,512]{1,0:T(8,128)(2,1)S(1)}, u32[]{:S(2)}, u32[]{:S(2)}) collective-permute-start(bf16[192,512]{1,0:T(8,128)(2,1)S(1)} %get-tuple-element.43), channel_id=1, source_target_pairs={{0,8},{8,16},{16,24},{24,0},{1,9},{9,17},{17,25},{25,1},{2,10},{10... | collective-permute-start | bytes 589832 | tf_op jit(solution)/shard_map/ppermute | solution.py:343
  67.8 16.6 %collective-permute-start.8 = (bf16[192,512]{1,0:T(8,128)(2,1)S(1)}, bf16[192,512]{1,0:T(8,128)(2,1)S(1)}, u32[]{:S(2)}, u32[]{:S(2)}) collective-permute-start(bf16[192,512]{1,0:T(8,128)(2,1)S(1)} %get-tuple-element.45), channel_id=1, source_target_pairs={{0,16},{8,24},{16,0},{24,8},{1,17},{9,25},{17,1},{25,9},{2,18},{10... | collective-permute-start | bytes 589832 | tf_op jit(solution)/shard_map/ppermute | solution.py:343
  69.4 15.1 %collective-permute-start.9 = (bf16[192,512]{1,0:T(8,128)(2,1)S(1)}, bf16[192,512]{1,0:T(8,128)(2,1)S(1)}, u32[]{:S(2)}, u32[]{:S(2)}) collective-permute-start(bf16[192,512]{1,0:T(8,128)(2,1)S(1)} %get-tuple-element.44), channel_id=1, source_target_pairs={{0,24},{8,0},{16,8},{24,16},{1,25},{9,1},{17,9},{25,17},{2,26},{10... | collective-permute-start | bytes 589832 | tf_op jit(solution)/shard_map/ppermute | solution.py:343
  76.9 6.6 %collective-permute-start.32 = (bf16[272,512]{1,0:T(8,128)(2,1)S(1)}, bf16[272,512]{1,0:T(8,128)(2,1)S(1)}, u32[]{:S(2)}, u32[]{:S(2)}) collective-permute-start(bf16[272,512]{1,0:T(8,128)(2,1)S(1)} %slice.35), channel_id=1, source_target_pairs={{0,4},{2,6},{4,0},{6,2},{1,5},{3,7},{5,1},{7,3},{8,12},{10,14},{12... | collective-permute-start | bytes 835592 | tf_op jit(solution)/shard_map/ppermute | solution.py:392
  79.5 26.5 %copy-start.15 = (bf16[528,512]{1,0:T(8,128)(2,1)}, bf16[528,512]{1,0:T(8,128)(2,1)S(1)}, u32[]{:S(2)}) copy-start(bf16[528,512]{1,0:T(8,128)(2,1)S(1)} %collective-permute-done.30.refs_2_) | copy-start | bytes 1622020
  83.6 0.7 copy-start.18
  84.4 32.9 %collective-permute-start.34 = (bf16[4,144,512]{2,1,0:T(8,128)(2,1)S(1)}, bf16[4,144,512]{2,1,0:T(8,128)(2,1)S(1)}, u32[]{:S(2)}, u32[]{:S(2)}) collective-permute-start(bf16[4,144,512]{2,1,0:T(8,128)(2,1)S(1)} %pad_maximum_fusion.1.refs_0_), channel_id=1, source_target_pairs={{0,1},{1,0},{2,3},{3,2},{4,5},{5,4},{6,7},{7,6},{8,9},{9,8},{10,11... | collective-permute-start | bytes 1769480 | tf_op jit(solution)/shard_map/ppermute | solution.py:481
  84.6 21.3 %copy-start.7 = (bf16[192,512]{1,0:T(8,128)(2,1)}, bf16[192,512]{1,0:T(8,128)(2,1)S(1)}, u32[]{:S(2)}) copy-start(bf16[192,512]{1,0:T(8,128)(2,1)S(1)} %add_convert_fusion.refs_3_.refs_5_) | copy-start | bytes 589828
  84.6 9.7 %collective-permute-start.13 = (bf16[192,512]{1,0:T(8,128)(2,1)S(1)}, bf16[192,512]{1,0:T(8,128)(2,1)S(1)}, u32[]{:S(2)}, u32[]{:S(2)}) collective-permute-start(bf16[192,512]{1,0:T(8,128)(2,1)S(1)} %add_convert_fusion.refs_3_.refs_5_), channel_id=1, source_target_pairs={{0,8},{8,16},{16,24},{24,0},{1,9},{9,17},{17,25},{25,1},{2,10},{10... | collective-permute-start | bytes 589832 | tf_op jit(solution)/shard_map/ppermute | solution.py:356
  87.7 14.7 %collective-permute-start.14 = (bf16[192,512]{1,0:T(8,128)(2,1)S(1)}, bf16[192,512]{1,0:T(8,128)(2,1)S(1)}, u32[]{:S(2)}, u32[]{:S(2)}) collective-permute-start(bf16[192,512]{1,0:T(8,128)(2,1)S(1)} %add_convert_fusion.refs_3_.refs_5_), channel_id=1, source_target_pairs={{0,16},{8,24},{16,0},{24,8},{1,17},{9,25},{17,1},{25,9},{2,18},{10... | collective-permute-start | bytes 589832 | tf_op jit(solution)/shard_map/ppermute | solution.py:356
  88.9 17.1 %collective-permute-start.33 = (bf16[256,256]{1,0:T(8,128)(2,1)S(1)}, bf16[256,256]{1,0:T(8,128)(2,1)S(1)}, u32[]{:S(2)}, u32[]{:S(2)}) collective-permute-start(bf16[256,256]{1,0:T(8,128)(2,1)S(1)} %get-tuple-element.36.refs_0_.a_ref), channel_id=1, source_target_pairs={{0,6},{2,4},{4,2},{6,0},{1,7},{3,5},{5,3},{7,1},{8,14},{10,12},{12... | collective-permute-start | bytes 393224 | tf_op jit(solution)/shard_map/ppermute | solution.py:429
  91.7 12.2 %collective-permute-start.15 = (bf16[192,512]{1,0:T(8,128)(2,1)S(1)}, bf16[192,512]{1,0:T(8,128)(2,1)S(1)}, u32[]{:S(2)}, u32[]{:S(2)}) collective-permute-start(bf16[192,512]{1,0:T(8,128)(2,1)S(1)} %add_convert_fusion.refs_3_.refs_5_), channel_id=1, source_target_pairs={{0,24},{8,0},{16,8},{24,16},{1,25},{9,1},{17,9},{25,17},{2,26},{10... | collective-permute-start | bytes 589832 | tf_op jit(solution)/shard_map/ppermute | solution.py:356
  94.3 11.9 %collective-permute-start.10 = (bf16[192,512]{1,0:T(8,128)(2,1)S(1)}, bf16[192,512]{1,0:T(8,128)(2,1)S(1)}, u32[]{:S(2)}, u32[]{:S(2)}) collective-permute-start(bf16[192,512]{1,0:T(8,128)(2,1)S(1)} %add_convert_fusion.refs_3_.refs_5_), channel_id=1, source_target_pairs={{0,2},{2,0},{4,6},{6,4},{1,3},{3,1},{5,7},{7,5},{8,10},{10,8},{12,... | collective-permute-start | bytes 589832 | tf_op jit(solution)/shard_map/ppermute | solution.py:360
  102.4 12.0 %collective-permute-start.11 = (bf16[192,512]{1,0:T(8,128)(2,1)S(1)}, bf16[192,512]{1,0:T(8,128)(2,1)S(1)}, u32[]{:S(2)}, u32[]{:S(2)}) collective-permute-start(bf16[192,512]{1,0:T(8,128)(2,1)S(1)} %add_convert_fusion.refs_3_.refs_5_), channel_id=1, source_target_pairs={{0,4},{2,6},{4,0},{6,2},{1,5},{3,7},{5,1},{7,3},{8,12},{10,14},{12... | collective-permute-start | bytes 589832 | tf_op jit(solution)/shard_map/ppermute | solution.py:360
  104.0 34.1 %collective-permute-start.12 = (bf16[192,512]{1,0:T(8,128)(2,1)S(1)}, bf16[192,512]{1,0:T(8,128)(2,1)S(1)}, u32[]{:S(2)}, u32[]{:S(2)}) collective-permute-start(bf16[192,512]{1,0:T(8,128)(2,1)S(1)} %add_convert_fusion.refs_3_.refs_5_), channel_id=1, source_target_pairs={{0,6},{2,4},{4,2},{6,0},{1,7},{3,5},{5,3},{7,1},{8,14},{10,12},{12... | collective-permute-start | bytes 589832 | tf_op jit(solution)/shard_map/ppermute | solution.py:360
  106.0 31.6 %copy-start.8 = (bf16[576,512]{1,0:T(8,128)(2,1)}, bf16[576,512]{1,0:T(8,128)(2,1)S(1)}, u32[]{:S(2)}) copy-start(bf16[576,512]{1,0:T(8,128)(2,1)S(1)} %shard_map.137.refs_9_) | copy-start | bytes 1769476
  106.0 35.7 %collective-permute-start.16 = (bf16[576,512]{1,0:T(8,128)(2,1)S(1)}, bf16[576,512]{1,0:T(8,128)(2,1)S(1)}, u32[]{:S(2)}, u32[]{:S(2)}) collective-permute-start(bf16[576,512]{1,0:T(8,128)(2,1)S(1)} %shard_map.137.refs_9_), channel_id=1, source_target_pairs={{0,2},{2,0},{4,6},{6,4},{1,3},{3,1},{5,7},{7,5},{8,10},{10,8},{12,... | collective-permute-start | bytes 1769480 | tf_op jit(solution)/shard_map/ppermute | solution.py:360
  106.2 31.3 %copy-start.22 = (bf16[192,512]{1,0:T(8,128)(2,1)}, bf16[192,512]{1,0:T(8,128)(2,1)S(1)}, u32[]{:S(2)}) copy-start(bf16[192,512]{1,0:T(8,128)(2,1)S(1)} %collective-permute-done.10.refs_6_) | copy-start | bytes 589828
  106.2 35.5 %collective-permute-start.17 = (bf16[576,512]{1,0:T(8,128)(2,1)S(1)}, bf16[576,512]{1,0:T(8,128)(2,1)S(1)}, u32[]{:S(2)}, u32[]{:S(2)}) collective-permute-start(bf16[576,512]{1,0:T(8,128)(2,1)S(1)} %shard_map.137.refs_9_), channel_id=1, source_target_pairs={{0,4},{2,6},{4,0},{6,2},{1,5},{3,7},{5,1},{7,3},{8,12},{10,14},{12... | collective-permute-start | bytes 1769480 | tf_op jit(solution)/shard_map/ppermute | solution.py:360
  114.4 23.2 %copy-start.23 = (bf16[192,512]{1,0:T(8,128)(2,1)}, bf16[192,512]{1,0:T(8,128)(2,1)S(1)}, u32[]{:S(2)}) copy-start(bf16[192,512]{1,0:T(8,128)(2,1)S(1)} %collective-permute-done.11.refs_7_) | copy-start | bytes 589828
  114.4 28.3 %collective-permute-start.18 = (bf16[576,512]{1,0:T(8,128)(2,1)S(1)}, bf16[576,512]{1,0:T(8,128)(2,1)}, u32[]{:S(2)}, u32[]{:S(2)}) collective-permute-start(bf16[576,512]{1,0:T(8,128)(2,1)S(1)} %shard_map.137.refs_9_), channel_id=1, source_target_pairs={{0,6},{2,4},{4,2},{6,0},{1,7},{3,5},{5,3},{7,1},{8,14},{10,12},{12... | collective-permute-start | bytes 1769480 | tf_op jit(solution)/shard_map/ppermute | solution.py:360
  117.2 24.5 %collective-permute-start.31 = (bf16[256,512]{1,0:T(8,128)(2,1)S(1)}, bf16[256,512]{1,0:T(8,128)(2,1)S(1)}, u32[]{:S(2)}, u32[]{:S(2)}) collective-permute-start(bf16[256,512]{1,0:T(8,128)(2,1)S(1)} %slice.34), channel_id=1, source_target_pairs={{0,2},{2,0},{4,6},{6,4},{1,3},{3,1},{5,7},{7,5},{8,10},{10,8},{12,... | collective-permute-start | bytes 786440 | tf_op jit(solution)/shard_map/ppermute | solution.py:391
  138.1 104.5 %copy-start.4 = (bf16[704,512]{1,0:T(8,128)(2,1)S(1)}, bf16[704,512]{1,0:T(8,128)(2,1)}, u32[]{:S(2)}) copy-start(bf16[704,512]{1,0:T(8,128)(2,1)} %copy-done.3) | copy-start | bytes 2162692
  138.1 104.5 %copy-start.6 = (bf16[704,512]{1,0:T(8,128)(2,1)S(1)}, bf16[704,512]{1,0:T(8,128)(2,1)}, u32[]{:S(2)}) copy-start(bf16[704,512]{1,0:T(8,128)(2,1)} %copy-done.5) | copy-start | bytes 2162692
  138.1 3.7 %copy-start.24 = (bf16[192,512]{1,0:T(8,128)(2,1)}, bf16[192,512]{1,0:T(8,128)(2,1)S(1)}, u32[]{:S(2)}) copy-start(bf16[192,512]{1,0:T(8,128)(2,1)S(1)} %collective-permute-done.12.refs_8_) | copy-start | bytes 589828
  141.7 3.6 %copy-start.21 = (bf16[256,512]{1,0:T(8,128)(2,1)}, bf16[256,512]{1,0:T(8,128)(2,1)S(1)}, u32[]{:S(2)}) copy-start(bf16[256,512]{1,0:T(8,128)(2,1)S(1)} %collective-permute-done.31.refs_3_) | copy-start | bytes 786436
  141.8 3.6 %copy-start.19 = (bf16[576,512]{1,0:T(8,128)(2,1)}, bf16[576,512]{1,0:T(8,128)(2,1)S(1)}, u32[]{:S(2)}) copy-start(bf16[576,512]{1,0:T(8,128)(2,1)S(1)} %collective-permute-done.16.refs_10_) | copy-start | bytes 1769476
  141.8 0.9 copy-start.20
  142.7 99.9 %collective-permute-start.35 = (bf16[1408,512]{1,0:T(8,128)(2,1)S(1)}, bf16[1408,512]{1,0:T(8,128)(2,1)S(1)}, u32[]{:S(2)}, u32[]{:S(2)}) collective-permute-start(bf16[1408,512]{1,0:T(8,128)(2,1)S(1)} %pad_maximum_fusion), channel_id=1, source_target_pairs={{0,6},{2,4},{4,2},{6,0},{1,7},{3,5},{5,3},{7,1},{8,14},{10,12},{12... | collective-permute-start | bytes 4325384 | tf_op jit(solution)/shard_map/ppermute | solution.py:507
  242.6 1.6 copy-start
  244.2 1.9 copy-start.16
  244.2 2.7 %copy-start.2 = (bf16[704,512]{1,0:T(8,128)(2,1)S(1)}, bf16[704,512]{1,0:T(8,128)(2,1)}, u32[]{:S(2)}) copy-start(bf16[704,512]{1,0:T(8,128)(2,1)} %copy-done.1) | copy-start | bytes 2162692
  246.0 2.7 %collective-permute-start.36 = (bf16[704,512]{1,0:T(8,128)(2,1)S(1)}, bf16[704,512]{1,0:T(8,128)(2,1)S(1)}, u32[]{:S(2)}, u32[]{:S(2)}) collective-permute-start(bf16[704,512]{1,0:T(8,128)(2,1)S(1)} %shard_map.146), channel_id=1, source_target_pairs={{0,1},{1,0},{2,3},{3,2},{4,5},{5,4},{6,7},{7,6},{8,9},{9,8},{10,11... | collective-permute-start | bytes 2162696 | tf_op jit(solution)/shard_map/ppermute | solution.py:509
  246.9 1.9 copy-start.13
  246.9 1.9 copy-start.14
